TPU v7x, 256 devices: a whole 4x4x8 slice. The times are simulated.
256 devices in a mesh: sp: 32 (over z, y), tp: 8 (over x, core).
Axes of the slice: x: 4, y: 4, z: 8, core: 2. Of those that a mesh axis runs over, the one named last changes fastest.
Arguments:
- tokens: bfloat16 [32768, 2048], P('sp'), may hold values from -6 to 6
- in_gain: float32 [2048], replicated, may hold values from 0.1 to 1.9
- w_query: bfloat16 [2048, 1024], P(None, 'tp'), may hold values from -0.125 to 0.125
- w_forget: bfloat16 [2048, 1024], P(None, 'tp'), may hold values from -0.125 to 0.125
- w_input: bfloat16 [2048, 1024], P(None, 'tp'), may hold values from -0.125 to 0.125
- w_outgate: bfloat16 [2048, 1024], P(None, 'tp'), may hold values from -0.125 to 0.125
- w_conv_h: bfloat16 [2048, 1024], P(None, 'tp'), may hold values from -0.125 to 0.125
- w_conv_b: bfloat16 [2048, 1024], P(None, 'tp'), may hold values from -0.125 to 0.125
- w_conv_c: bfloat16 [2048, 1024], P(None, 'tp'), may hold values from -0.125 to 0.125
- forget_floor: float32 [1024], P('tp'), may hold values from 0.84 to 1
- forget_leak: float32 [32768, 1024], P('sp', 'tp'), may hold values from -1 to 0
- state_gain: float32 [128], replicated, may hold values from 0.1 to 1.9
- conv_taps: bfloat16 [3, 1024], P(None, 'tp'), may hold values from -3.5 to 3.5
- group_gain: float32 [128], replicated, may hold values from 0.1 to 1.9
- out_state: bfloat16 [1024, 2048], P('tp'), may hold values from -0.1875 to 0.1875
- out_conv: bfloat16 [1024, 2048], P('tp'), may hold values from -0.1875 to 0.1875
Outputs:
- mixed_out: bfloat16 [32768, 2048], P('sp', 'tp')
All inputs are finite; a program needn't handle non-finite values.
Results may differ from a plain program's by a relative error of at most 0.015.
Values may be sent and summed in bfloat16 or wider, within the bound.
A program may use at most 128 MiB of HBM per device.

v0:
```python
import jax
import jax.numpy as jnp
from jax import lax
from jax.sharding import Mesh
from jax.sharding import PartitionSpec as P

GROUP_FEATURES = 128
BLOCK = 64
TAPS = 3
SP = ("sp_0", "sp_1")


norm_eps = 1e-06


def from_behind(array, axis, by):
    count = lax.axis_size(axis)
    pairs = [(i, i + by) for i in range(count) if 0 <= i + by < count]
    return lax.ppermute(array, axis, pairs)


def neutral_like(array, identity):
    return jax.tree.map(
        lambda part, zero: jnp.zeros_like(part) + jnp.asarray(zero, part.dtype), array, identity
    )


def collected_together(array, axis):
    leaves = jax.tree.leaves(array)
    turns = sorted(range(len(leaves)), key=lambda k: -leaves[k].size)
    width = (1, *leaves[turns[0]].shape)[-1]
    lines = [
        jnp.pad(leaves[k].reshape(-1), (0, -leaves[k].size % width)).reshape(-1, width)
        for k in turns
    ]
    both, at, found = (lax.all_gather(jnp.concatenate(lines), axis), 0, {})
    for k, line in zip(turns, lines):
        section = both[:, at : at + len(line)].reshape(len(both), -1)
        found[k] = section[:, : leaves[k].size].reshape(-1, *leaves[k].shape)
        at += len(line)
    numbers = iter(range(len(leaves)))
    return jax.tree.map(lambda _: found[next(numbers)], array)


def carried_in(array, axes, combine, identity):
    before = start = neutral_like(array, identity)
    subtotal = array
    for axis in reversed(axes):
        count, index = (lax.axis_size(axis), lax.axis_index(axis))
        pieces = collected_together(
            jax.tree.map(
                lambda part, kind: part.astype(kind), subtotal, (jnp.bfloat16, jnp.bfloat16)
            ),
            axis,
        )
        inside, subtotal = (start, start)
        for k in range(count):
            passed = k < index
            subtotal = combine(
                subtotal, jax.tree.map(lambda part, own: part[k].astype(own.dtype), pieces, array)
            )
            inside = jax.tree.map(lambda new, old: jnp.where(passed, new, old), subtotal, inside)
        before = combine(inside, before)
    return before


def rms_rows(values, gain):
    scale = lax.rsqrt(jnp.mean(values * values, axis=-1, keepdims=True) + norm_eps)
    return values * scale * gain


def state_block(carry, inputs):
    carry_state, offset = carry
    query_blk, key_blk, value_blk, logf_blk = inputs
    cum_log = jnp.cumsum(logf_blk, axis=1)
    carried = jnp.einsum("hcd,hde->hce", query_blk * jnp.exp(cum_log), carry_state)
    length = logf_blk.shape[1]
    causal = (jnp.arange(length)[:, None] >= jnp.arange(length)[None, :])[None, :, :, None]
    diff_log = cum_log[:, :, None, :] - cum_log[:, None, :, :]
    decay_all = jnp.exp(jnp.where(causal, diff_log, -jnp.inf))
    scores = jnp.einsum("hid,hjd,hijd->hij", query_blk, key_blk, decay_all)
    result = carried + jnp.einsum("hij,hje->hie", scores, value_blk)
    last_log = cum_log[:, -1, :]
    fresh = jnp.einsum("hcd,hce->hde", key_blk * jnp.exp(last_log[:, None, :] - cum_log), value_blk)
    new_state = jnp.exp(last_log)[:, :, None] * carry_state + fresh
    return ((new_state, offset + last_log), (result, offset[:, None, :] + cum_log))


def join_states(earlier, later):
    earlier_log, earlier_state = earlier
    later_log, later_state = later
    return (earlier_log + later_log, jnp.exp(later_log)[:, :, None] * earlier_state + later_state)


def body(
    tokens,
    in_gain,
    w_query,
    w_forget,
    w_input,
    w_outgate,
    w_conv_h,
    w_conv_b,
    w_conv_c,
    forget_floor,
    forget_leak,
    state_gain,
    conv_taps,
    group_gain,
    out_state,
    out_conv,
):
    count = tokens.shape[0]
    heads = w_query.shape[1] // GROUP_FEATURES
    channels = w_conv_h.shape[1]
    normed = rms_rows(tokens.astype(jnp.float32), in_gain).astype(jnp.bfloat16)

    def project(weight):
        return jnp.dot(normed, weight, preferred_element_type=jnp.float32).astype(jnp.bfloat16)

    proj_query = project(w_query)
    proj_forget = project(w_forget)
    proj_input = project(w_input)
    proj_outgate = project(w_outgate)
    proj_h = project(w_conv_h)
    proj_b = project(w_conv_b)
    proj_c = project(w_conv_c)
    conv_in = (proj_c.astype(jnp.float32) * proj_h.astype(jnp.float32)).astype(jnp.bfloat16)
    rim_rows = from_behind(conv_in[count - (TAPS - 1) :], SP, 1)
    gate_logit = proj_forget.astype(jnp.float32)
    log_forget = (
        jnp.logaddexp(
            jnp.log(forget_floor), jnp.log1p(-forget_floor) + jax.nn.log_sigmoid(gate_logit)
        )
        + forget_leak
    )
    key_gate = (1.0 - forget_floor) * jax.nn.sigmoid(-gate_logit)
    query_act = jax.nn.silu(proj_query.astype(jnp.float32))
    value_f = proj_input.astype(jnp.float32)
    nblk = count // BLOCK

    def to_blocks(arr):
        return arr.reshape(nblk, BLOCK, heads, GROUP_FEATURES).transpose(0, 2, 1, 3)

    def from_blocks(arr):
        return arr.transpose(0, 2, 1, 3).reshape(count, heads, GROUP_FEATURES)

    start_state = jnp.zeros((heads, GROUP_FEATURES, GROUP_FEATURES), jnp.float32)
    start_log = jnp.zeros((heads, GROUP_FEATURES), jnp.float32)
    (local_state, total_log), (local_read, cum_blocks) = lax.scan(
        state_block,
        (start_state, start_log),
        (to_blocks(query_act), to_blocks(key_gate), to_blocks(value_f), to_blocks(log_forget)),
    )
    _, incoming = carried_in((total_log, local_state), SP, join_states, (start_log, start_state))
    cum_device = from_blocks(cum_blocks)
    query_heads = query_act.reshape(count, heads, GROUP_FEATURES)
    cross = jnp.einsum("thd,hde->the", query_heads * jnp.exp(cum_device), incoming)
    state_read = from_blocks(local_read) + cross
    out_gate = jax.nn.silu(proj_outgate.astype(jnp.float32)).reshape(count, heads, GROUP_FEATURES)
    state_res = (
        (rms_rows(state_read, state_gain) * out_gate)
        .reshape(count, heads * GROUP_FEATURES)
        .astype(jnp.bfloat16)
    )
    padded = jnp.concatenate([rim_rows, conv_in], axis=0).astype(jnp.float32)
    taps_f = conv_taps.astype(jnp.float32)
    conv_sum = jnp.zeros((count, channels), jnp.float32)
    for offset in range(TAPS):
        conv_sum = conv_sum + taps_f[offset][None, :] * padded[offset : offset + count]
    gated = (proj_b.astype(jnp.float32) * conv_sum).reshape(
        count, channels // GROUP_FEATURES, GROUP_FEATURES
    )
    conv_res = rms_rows(gated, group_gain).reshape(count, channels).astype(jnp.bfloat16)
    mixed_here = jnp.concatenate([state_res, conv_res], axis=1)
    weight_rows = jnp.concatenate([out_state, out_conv], axis=0)
    columns = lax.all_to_all(weight_rows, "tp", split_axis=1, concat_axis=0, tiled=True)
    summed = jnp.dot(
        lax.all_gather(mixed_here, "tp", axis=1, tiled=True),
        columns,
        preferred_element_type=jnp.float32,
    )
    return summed.astype(jnp.bfloat16)


def solution(mesh):
    split = Mesh(mesh.devices.reshape(8, 4, mesh.shape["tp"]), ("sp_0", "sp_1", "tp"))
    placed = (
        P(SP, None),
        P(),
        P(None, "tp"),
        P(None, "tp"),
        P(None, "tp"),
        P(None, "tp"),
        P(None, "tp"),
        P(None, "tp"),
        P(None, "tp"),
        P("tp"),
        P(SP, "tp"),
        P(),
        P(None, "tp"),
        P(),
        P("tp", None),
        P("tp", None),
    )
    return jax.shard_map(body, mesh=split, in_specs=placed, out_specs=P(SP, "tp"), check_vma=False)
```

profile of v0, /device:TPU:1, one launch (start us, length us, event | category | flops | bytes accessed | tf_op | source)
XLA Modules:
  0.0 187.0 jit_solution(12285283551542501446)
XLA Ops:
  6.5 3.2 %fusion.30 = f32[1024]{0:T(1024)S(1)} fusion(bf16[1024,2048]{1,0:T(8,128)(2,1)} %param.18), kind=kLoop, calls=%fused_computation.44 | loop fusion | flops 6290432 | bytes 4198400 | tf_op jit(solution)/shard_map/reduce_sum | solution.py:68
  11.1 1.2 fusion.37
  12.5 1.3 fusion.36
  13.8 4.0 %collective-permute-start = (bf16[2,128]{1,0:T(2,128)(2,1)S(1)}, bf16[2,128]{1,0:T(2,128)(2,1)S(1)}, u32[]{:S(2)}, u32[]{:S(2)}) collective-permute-start(bf16[2,128]{1,0:T(2,128)(2,1)S(1)} %slice.193), channel_id=1, source_target_pairs={{0,8},{8,16},{16,24},{24,32},{32,40},{40,48},{48,56},{56,64},{64,7... | collective-permute-start | bytes 1544 | tf_op jit(solution)/shard_map/ppermute | solution.py:19
  18.0 3.6 %divide_multiply_fusion = f32[1024,128]{1,0:T(8,128)S(1)} fusion(bf16[1024,2048]{1,0:T(8,128)(2,1)} %copy-done.1, bf16[2048,128]{1,0:T(8,128)(2,1)S(1)} %copy-done.13), kind=kOutput, calls=%fused_computation.83 | convolution fusion | flops 537657344 | bytes 5242880 | tf_op jit(solution)/shard_map/dot_general | solution.py:119
  21.6 1.2 convolution_convert_fusion.6
  22.9 1.8 divide_multiply_fusion.1
  24.6 58.7 %while.17 = (s32[]{:T(128)}, f32[1,128,128]{2,1,0:T(8,128)S(1)}, f32[1,128]{1,0:T(1,128)S(1)}, f32[16,1,64,128]{3,2,1,0:T(8,128)}, f32[16,1,64,128]{3,2,1,0:T(8,...) while((s32[]{:T(128)}, f32[1,128,128]{2,1,0:T(8,128)S(1)}, ...), condition=%wide.region_3.4_spmd.clone, body=%wide.region_1.3_spmd.clone.sunk | while | flops 8487171 | bytes 5119637 | solution.py:150
  25.4 1.7 fusion.189
  29.1 1.7 fusion.189
  32.8 1.7 fusion.189
  36.4 1.7 fusion.189
  40.1 1.7 fusion.189
  43.8 1.7 fusion.189
  47.4 1.7 fusion.189
  51.1 1.7 fusion.189
  54.8 1.7 fusion.189
  58.4 1.7 fusion.189
  62.1 1.7 fusion.189
  65.8 1.7 fusion.189
  69.4 1.7 fusion.189
  73.1 1.7 fusion.189
  76.8 1.7 fusion.189
  80.4 1.7 fusion.189
  83.4 9.5 %all-gather.2 = bf16[4,129,128]{2,1,0:T(8,128)(2,1)S(1)} all-gather(bf16[1,129,128]{2,1,0:T(8,128)(2,1)S(1)} %maximum_bitcast_fusion), channel_id=2, replica_groups=mesh['sp_0'=8,'sp_1'=4,'tp'=8] {'sp_1'}, dimensions={0}, use_global_device_ids=true | all-gather | bytes 165120 | tf_op jit(solution)/shard_map/all_gather | solution.py:36
  93.1 22.4 %all-gather.3 = bf16[8,129,128]{2,1,0:T(8,128)(2,1)S(1)} all-gather(bf16[1,129,128]{2,1,0:T(8,128)(2,1)S(1)} %maximum_bitcast_fusion.1), channel_id=3, replica_groups=mesh['sp_0'=8,'sp_1'=4,'tp'=8] {'sp_0'}, dimensions={0}, use_global_device_ids=true | all-gather | bytes 297216 | tf_op jit(solution)/shard_map/all_gather | solution.py:36
  115.6 1.7 multiply_reduce_fusion.1
  117.4 3.6 %fusion.48 = bf16[1024,128]{1,0:T(8,128)(2,1)S(1)} fusion(bf16[1024,2048]{1,0:T(8,128)(2,1)} %copy-done.1, bf16[2048,128]{1,0:T(8,128)(2,1)S(1)} %copy-done.16, f32[1024,1,128]{2,0,1:T(8,128)S(1)} %get-tuple-element.181, f32[128]{0:T(128)S(1)} %copy-done.18, f32[1024]{0:T(1024)S(1)} %add_rsqrt_fusion.1), kind=kOutput, calls=%fused_computation.81 | convolution fusion | flops 538181632 | bytes 5509632 | tf_op jit(solution)/shard_map/dot_general | solution.py:119
  121.2 1.3 multiply_reduce_fusion
  124.3 34.8 %all_to_all.19 = bf16[256,8,256]{0,2,1:T(8,128)(2,1)S(1)} all-to-all(bf16[256,8,256]{0,2,1:T(8,128)(2,1)S(1)} %bitcast.205), channel_id=1, replica_groups=mesh['sp_0'=8,'sp_1'=4,'tp'=8] {'tp'}, dimensions={1} | all-to-all | bytes 2097152 | tf_op jit(solution)/shard_map/all_to_all | solution.py:177
  159.6 16.3 %all-gather.6.cloned.1.call-done = bf16[1024,2048]{1,0:T(8,128)(2,1)} async-done(((bf16[1024,256]{1,0:T(8,128)(2,1)}), bf16[1024,2048]{1,0:T(8,128)(2,1)}) %all-gather.6.cloned.1.call-update) | async-done | bytes 4194320 | tf_op jit(solution)/shard_map/all_gather | solution.py:179
  176.0 4.2 %convolution_convert_fusion = bf16[1024,256]{1,0:T(8,128)(2,1)} fusion(bf16[1024,2048]{1,0:T(8,128)(2,1)} %all-gather.6.cloned.1.call-done, bf16[2048,256]{1,0:T(8,128)(2,1)S(1)} %bitcast.209), kind=kOutput, calls=%fused_computation.48 | convolution fusion | flops 1074003968 | bytes 5767168 | tf_op jit(solution)/shard_map/dot_general | solution.py:178
  (261 shorter events, 34.6 us)
Async XLA Ops:
  6.5 16.3 %copy-start = (bf16[2048,128]{1,0:T(8,128)(2,1)S(1)}, bf16[2048,128]{1,0:T(8,128)(2,1)}, u32[]{:S(2)}) copy-start(bf16[2048,128]{1,0:T(8,128)(2,1)} %param.21) | copy-start | bytes 1572868
  6.5 3.2 %copy-start.9 = (f32[2048]{0:T(1024)S(1)}, f32[2048]{0:T(1024)}, u32[]{:S(2)}) copy-start(f32[2048]{0:T(1024)} %param.19) | copy-start | bytes 24580
  6.5 169.4 %all-gather.6.cloned.1.call-start = ((), (), s32[]{:S(2)}) async-start(), calls=%async_computation.1 | async-start | bytes 4718592 | tf_op jit(solution)/shard_map/all_gather | solution.py:179
  6.5 3.5 %copy-start.4 = (bf16[1024,2048]{1,0:T(8,128)(2,1)S(1)}, bf16[1024,2048]{1,0:T(8,128)(2,1)}, u32[]{:S(2)}) copy-start(bf16[1024,2048]{1,0:T(8,128)(2,1)} %param.18) | copy-start | bytes 12582916
  10.1 1.0 copy-start.5
  11.1 2.7 %copy-start.1 = (bf16[1024,2048]{1,0:T(8,128)(2,1)}, bf16[1024,2048]{1,0:T(8,128)(2,1)S(1)}, u32[]{:S(2)}) copy-start(bf16[1024,2048]{1,0:T(8,128)(2,1)S(1)} %fusion.32) | copy-start | bytes 12582916
  11.1 1.4 copy-start.6
  12.5 5.4 %copy-start.11 = (f32[128]{0:T(128)S(1)}, f32[128]{0:T(128)}, u32[]{:S(2)}) copy-start(f32[128]{0:T(128)} %param.27) | copy-start | bytes 1540
  12.5 5.4 %copy-start.13 = (bf16[2048,128]{1,0:T(8,128)(2,1)S(1)}, bf16[2048,128]{1,0:T(8,128)(2,1)}, u32[]{:S(2)}) copy-start(bf16[2048,128]{1,0:T(8,128)(2,1)} %param.20) | copy-start | bytes 1572868
  13.8 107.2 %collective-permute-start = (bf16[2,128]{1,0:T(2,128)(2,1)S(1)}, bf16[2,128]{1,0:T(2,128)(2,1)S(1)}, u32[]{:S(2)}, u32[]{:S(2)}) collective-permute-start(bf16[2,128]{1,0:T(2,128)(2,1)S(1)} %slice.193), channel_id=1, source_target_pairs={{0,8},{8,16},{16,24},{24,32},{32,40},{40,48},{48,56},{56,64},{64,7... | collective-permute-start | bytes 1544 | tf_op jit(solution)/shard_map/ppermute | solution.py:19
  17.9 3.6 %copy-start.2 = (bf16[1024,2048]{1,0:T(8,128)(2,1)S(1)}, bf16[1024,2048]{1,0:T(8,128)(2,1)}, u32[]{:S(2)}) copy-start(bf16[1024,2048]{1,0:T(8,128)(2,1)} %copy-done.1) | copy-start | bytes 12582916
  18.0 3.6 %copy-start.14 = (bf16[2048,128]{1,0:T(8,128)(2,1)S(1)}, bf16[2048,128]{1,0:T(8,128)(2,1)}, u32[]{:S(2)}) copy-start(bf16[2048,128]{1,0:T(8,128)(2,1)} %param.22) | copy-start | bytes 1572868
  21.6 1.3 copy-start.15
  83.3 34.0 %copy-start.10 = (bf16[3,128]{1,0:T(4,128)(2,1)S(1)}, bf16[3,128]{1,0:T(4,128)(2,1)}, u32[]{:S(2)}) copy-start(bf16[3,128]{1,0:T(4,128)(2,1)} %param.30) | copy-start | bytes 2308
  83.4 34.1 %copy-start.16 = (bf16[2048,128]{1,0:T(8,128)(2,1)S(1)}, bf16[2048,128]{1,0:T(8,128)(2,1)}, u32[]{:S(2)}) copy-start(bf16[2048,128]{1,0:T(8,128)(2,1)} %param.23) | copy-start | bytes 1572868
  83.4 34.1 %copy-start.18 = (f32[128]{0:T(128)S(1)}, f32[128]{0:T(128)}, u32[]{:S(2)}) copy-start(f32[128]{0:T(128)} %param.29) | copy-start | bytes 1540
  117.4 3.7 %copy-start.3 = (bf16[1024,2048]{1,0:T(8,128)(2,1)S(1)}, bf16[1024,2048]{1,0:T(8,128)(2,1)}, u32[]{:S(2)}) copy-start(bf16[1024,2048]{1,0:T(8,128)(2,1)} %copy-done.1) | copy-start | bytes 12582916
  117.4 3.7 %copy-start.17 = (bf16[2048,128]{1,0:T(8,128)(2,1)S(1)}, bf16[2048,128]{1,0:T(8,128)(2,1)}, u32[]{:S(2)}) copy-start(bf16[2048,128]{1,0:T(8,128)(2,1)} %param.25) | copy-start | bytes 1572868
  121.2 1.4 copy-start.12
  121.2 2.5 %copy-start.7 = (bf16[128,2048]{1,0:T(8,128)(2,1)S(1)}, bf16[128,2048]{1,0:T(8,128)(2,1)}, u32[]{:S(2)}) copy-start(bf16[128,2048]{1,0:T(8,128)(2,1)} %param.32) | copy-start | bytes 1572868
  121.2 2.7 %copy-start.8 = (bf16[128,2048]{1,0:T(8,128)(2,1)S(1)}, bf16[128,2048]{1,0:T(8,128)(2,1)}, u32[]{:S(2)}) copy-start(bf16[128,2048]{1,0:T(8,128)(2,1)} %param.33) | copy-start | bytes 1572868
Sparse Core Ops, SparseCore 0:
  123.8 52.1 all-gather.5
where the time goes:
time: 187 us
  blocking collectives  66.6 us (36%)
  other arithmetic  44.8 us (24%)
  matrix products  38.1 us (20%)
  waiting for transfers between devices  16.4 us (9%)
  between operations  13.9 us (7%)
  starting transfers between devices  4.02 us (2%)
  local copies, waits for them, and re-layouts  2.2 us (1%)
    all_to_all x1, blocking collectives, body(): lax.all_to_all(weight_rows, 'tp', split_axis=1, concat_axis=0, tiled=True)  34.8 us
    all_gather x2, blocking collectives, collected_together(): both, at, found = (lax.all_gather(jnp.concatenate(lines), axis), 0, {})  31.9 us
    dot_general x16, other arithmetic, state_block(): scores = jnp.einsum('hid,hjd,hijd->hij', query_blk, key_blk, decay_all)  27.3 us
    all_gather x1, waiting for transfers between devices, body(): lax.all_gather(mixed_here, 'tp', axis=1, tiled=True)  16.3 us
    dot_general x7, matrix products, project(): jnp.dot(normed, weight, preferred_element_type=jnp.float32)  14 us
    dot_general x16, matrix products, state_block(): result = carried + jnp.einsum('hij,hje->hie', scores, value_blk)  12.7 us
    exp x16, other arithmetic, state_block(): decay_all = jnp.exp(jnp.where(causal, diff_log, -jnp.inf))  9.79 us
    dot_general x1, matrix products, body(): jnp.dot(lax.all_gather(mixed_here, 'tp', axis=1, tiled=True), columns, pr...  4.23 us
  transfers between devices with their start and end apart: 2, of which 1 were waited for; matrix products, arithmetic and copies ran while one was open for 38% of the time, Pallas kernels for 0%

commit v1 on v0

v1 whole, which is shorter than its diff:
```python
import functools

import jax
import jax.numpy as jnp
from jax import lax
from jax.experimental import pallas as pl
from jax.experimental.pallas import tpu as pltpu
from jax.sharding import Mesh
from jax.sharding import PartitionSpec as P

G = 128
PAD = 8
NORM_EPS = 1e-06
MESH = pl.DeviceIdType.MESH
bf16, f32 = jnp.bfloat16, jnp.float32


def dot(a, b):
    return jnp.dot(a, b, preferred_element_type=f32)


def dot_nt(a, b):
    return lax.dot_general(a, b, (((1,), (1,)), ((), ())), preferred_element_type=f32)


def dot_tn(a, b):
    return lax.dot_general(a, b, (((0,), (0,)), ((), ())), preferred_element_type=f32)


def sigmoid(v):
    return 1.0 / (1.0 + jnp.exp(-v))


def rounded(v):
    return v.astype(bf16).astype(f32)


def split3(v):
    h1 = v.astype(bf16)
    r1 = v - h1.astype(f32)
    h2 = r1.astype(bf16)
    h3 = (r1 - h2.astype(f32)).astype(bf16)
    return h1, h2, h3


def kernel(
    sizes,
    tokens, in_gain, w_query, w_forget, w_input, w_outgate, w_conv_h, w_conv_b, w_conv_c,
    floor, leak, state_gain, taps, group_gain, out_state, out_conv,
    out,
    tok_v, w_v, leak_v, prior_v, offs_v, qin_v, oa_v, gate_v, cin_v, pb_v,
    gath_c, gath_s, wcol_c, wcol_s, acc_v, out_v,
    a_src, a_recv, b_src, b_recv, c_src, c_recv,
    tok_sem, w_sem, leak_sem, own_sem, out_sem,
    ws_sem, wr_sem, as_sem, ar_sem, bs_sem, br_sem, cs_sem, cr_sem, rim_sem,
    gs_sem, gr_sem,
):
    Z, Y, X, C = sizes
    TP = X * C
    T = tok_v.shape[0]
    N = T // G
    BIG = 2 * G
    NB = T // BIG
    Q = G // Y
    COLS = out_v.shape[1]
    z, y, x, c = (lax.axis_index(n) for n in ("z", "y", "x", "core"))
    me = x * C + c
    other = 1 - c
    right, left = lax.rem(x + 1, X), lax.rem(x + X - 1, X)
    far = lax.rem(x + 2, X)

    def at(**kw):
        where = {"z": z, "y": y, "x": x, "core": c}
        where.update(kw)
        return (where["z"], where["y"], where["x"], where["core"])

    def lanes(src):
        return pl.ds(pl.multiple_of(src * G, G), G)

    tok_in = [
        pltpu.make_async_copy(tokens.at[pl.ds(k * BIG, BIG)], tok_v.at[pl.ds(k * BIG, BIG)], tok_sem.at[k])
        for k in range(NB)
    ]
    weights = (w_forget, w_input, w_query, w_outgate, w_conv_h, w_conv_c, w_conv_b)
    w_in = [
        pltpu.make_async_copy(w, w_v.at[:, pl.ds(k * G, G)], w_sem.at[k]) for k, w in enumerate(weights)
    ]
    leak_in = pltpu.make_async_copy(leak, leak_v, leak_sem)
    tok_in[0].start()
    for k in range(4):
        w_in[k].start()
    leak_in.start()
    for k in range(1, NB):
        tok_in[k].start()
    for k in range(4, 7):
        w_in[k].start()
    own_in = []
    for k, (src, dst) in enumerate(((out_state, wcol_s), (out_conv, wcol_c))):
        cp = pltpu.make_async_copy(
            src.at[:, pl.ds(pl.multiple_of(me * COLS, COLS), COLS)],
            dst.at[pl.ds(pl.multiple_of(me * G, G), G), :],
            own_sem.at[k],
        )
        cp.start()
        own_in.append(cp)

    barrier = pltpu.get_barrier_semaphore()
    for d in range(1, TP):
        t = lax.rem(me + d, TP)
        pl.semaphore_signal(barrier, inc=1, device_id=at(x=t // C, core=lax.rem(t, C)), device_id_type=MESH)
    for d in range(1, Y):
        pl.semaphore_signal(barrier, inc=1, device_id=at(y=lax.rem(y + d, Y)), device_id_type=MESH)
    for d in range(1, Z):
        pl.semaphore_signal(barrier, inc=1, device_id=at(z=lax.rem(z + d, Z)), device_id_type=MESH)
    last_y, first_y = y == Y - 1, y == 0

    @pl.when(last_y)
    def _():
        pl.semaphore_signal(barrier, inc=1, device_id=at(z=lax.rem(z + 1, Z), y=0), device_id_type=MESH)

    @pl.when(first_y)
    def _():
        pl.semaphore_signal(barrier, inc=1, device_id=at(z=lax.rem(z + Z - 1, Z), y=Y - 1), device_id_type=MESH)

    count = TP - 1 + Y - 1 + Z - 1
    at_rim = jnp.logical_or(last_y, first_y)

    @pl.when(at_rim)
    def _():
        pl.semaphore_wait(barrier, count + 1)

    @pl.when(jnp.logical_not(at_rim))
    def _():
        pl.semaphore_wait(barrier, count)

    def w_copy(part, d):
        t = lax.rem(me + d, TP)
        src, dst = ((out_state, wcol_s), (out_conv, wcol_c))[part]
        return pltpu.make_async_remote_copy(
            src_ref=src.at[:, pl.ds(pl.multiple_of(t * COLS, COLS), COLS)],
            dst_ref=dst.at[pl.ds(pl.multiple_of(me * G, G), G), :],
            send_sem=ws_sem.at[part, d],
            recv_sem=wr_sem.at[part, d],
            device_id=at(x=t // C, core=lax.rem(t, C)),
            device_id_type=MESH,
        )

    for part in (1, 0):
        for d in range(1, TP):
            w_copy(part, d).start()

    gain_in = in_gain[...]
    fl = floor[...]
    row_i = lax.broadcasted_iota(jnp.int32, (G, G), 0)
    col_i = lax.broadcasted_iota(jnp.int32, (G, G), 1)
    lower = row_i >= col_i
    tri = jnp.where(lower, 1.0, 0.0).astype(bf16)

    def norm_rows(k):
        def step(i, _):
            rows = pl.ds(pl.multiple_of(k * BIG + i * 16, 16), 16)
            v = tok_v[rows, :].astype(f32)
            s = lax.rsqrt(jnp.mean(v * v, axis=-1, keepdims=True) + NORM_EPS)
            tok_v[rows, :] = (v * s * gain_in).astype(bf16)
            return 0

        lax.fori_loop(0, BIG // 16, step, 0, unroll=2)

    state = jnp.zeros((G, G), f32)
    offset = jnp.zeros((1, G), f32)
    for k in range(NB):
        tok_in[k].wait()
        norm_rows(k)
        if k == 0:
            for j in range(4):
                w_in[j].wait()
            leak_in.wait()
        big = pl.ds(k * BIG, BIG)
        proj = dot(tok_v[big, :], w_v[:, 0 : 4 * G])
        for h in range(2):
            n = 2 * k + h
            rows = pl.ds(n * G, G)
            pf = rounded(proj[h * G : (h + 1) * G, 0:G])
            pi = proj[h * G : (h + 1) * G, G : 2 * G].astype(bf16)
            pq = rounded(proj[h * G : (h + 1) * G, 2 * G : 3 * G])
            po = rounded(proj[h * G : (h + 1) * G, 3 * G : 4 * G])
            key = (1.0 - fl) * sigmoid(-pf)
            logf = jnp.log1p(-key) + leak_v[rows, :]
            query = pq * sigmoid(pq)
            gate_v[rows, :] = po * sigmoid(po)
            h1, h2, h3 = split3(logf)
            cum3 = dot(tri, jnp.concatenate([h1, h2, h3], axis=1))
            cum = cum3[:, 0:G] + cum3[:, G : 2 * G] + cum3[:, 2 * G : 3 * G]
            mid, last = cum[G // 2 - 1 : G // 2, :], cum[G - 1 : G, :]
            q_mid = query * jnp.exp(cum - mid)
            k_mid = key * jnp.exp(mid - cum)
            scores = jnp.where(lower, dot_nt(q_mid.astype(bf16), k_mid.astype(bf16)), 0.0)
            oa_v[rows, :] = dot(scores.astype(bf16), pi)
            qin_v[rows, :] = (q_mid * jnp.exp(mid)).astype(bf16)
            prior_v[n] = state
            offs_v[n] = jnp.broadcast_to(jnp.exp(offset), (8, G))
            k_last = (k_mid * jnp.exp(last - mid)).astype(bf16)
            state = state * jnp.exp(last) + dot_tn(pi, k_last)
            offset = offset + last

    def decay_rows(decay):
        hi = decay.astype(bf16).astype(f32)
        r = lax.broadcasted_iota(jnp.int32, (16, G), 0)
        return jnp.where(r == 0, hi, jnp.where(r == 1, decay - hi, 0.0)).astype(bf16)

    def piece(ref, slot):
        block = ref[slot].astype(f32)
        return block[0:Q, :], block[Q : Q + 1, :] + block[Q + 1 : Q + 2, :]

    extra = decay_rows(jnp.exp(offset))
    for j in range(Y):
        a_src[j, 0:Q, :] = state[j * Q : (j + 1) * Q, :].astype(bf16)
        a_src[j, Q : Q + 16, :] = extra
    a_recv[y] = a_src[y]

    def a_copy(d):
        t = lax.rem(y + d, Y)
        return pltpu.make_async_remote_copy(
            src_ref=a_src.at[t], dst_ref=a_recv.at[y], send_sem=as_sem.at[d], recv_sem=ar_sem.at[d],
            device_id=at(y=t), device_id_type=MESH,
        )

    for d in range(1, Y):
        a_copy(d).start()

    for j in range(4, 7):
        w_in[j].wait()

    def conv_proj(k):
        big = pl.ds(k * BIG, BIG)
        proj = dot(tok_v[big, :], w_v[:, 4 * G : 7 * G])
        ph, pc = rounded(proj[:, 0:G]), rounded(proj[:, G : 2 * G])
        pb_v[big, :] = rounded(proj[:, 2 * G : 3 * G])
        cin_v[pl.ds(PAD + k * BIG, BIG), :] = rounded(pc * ph)

    conv_proj(NB - 1)
    is_first = jnp.logical_and(z == 0, y == 0)
    is_last = jnp.logical_and(z == Z - 1, y == Y - 1)
    carry = lax.select(last_y, 1, 0)
    rim = pltpu.make_async_remote_copy(
        src_ref=cin_v.at[pl.ds(T, PAD)], dst_ref=cin_v.at[pl.ds(0, PAD)],
        send_sem=rim_sem.at[0], recv_sem=rim_sem.at[1],
        device_id=at(z=lax.rem(z + carry, Z), y=lax.rem(y + 1, Y)), device_id_type=MESH,
    )

    @pl.when(jnp.logical_not(is_last))
    def _():
        rim.start()

    @pl.when(is_first)
    def _():
        cin_v[0:PAD, :] = jnp.zeros((PAD, G), f32)

    conv_proj(0)

    for d in range(1, Y):
        a_copy(d).wait_recv()
    total, total_d = piece(a_recv, 0)
    for j in range(1, Y):
        s, dec = piece(a_recv, j)
        total, total_d = total * dec + s, total_d * dec
    b_src[0:Q, :] = total.astype(bf16)
    b_src[Q : Q + 16, :] = decay_rows(total_d)

    def b_copy(d):
        return pltpu.make_async_remote_copy(
            src_ref=b_src, dst_ref=b_recv.at[z], send_sem=bs_sem.at[d], recv_sem=br_sem.at[d],
            device_id=at(z=lax.rem(z + d, Z)), device_id_type=MESH,
        )

    for d in range(1, Z):
        @pl.when(z + d < Z)
        def _():
            b_copy(d).start()

    for k in range(1, NB - 1):
        conv_proj(k)

    @pl.when(jnp.logical_not(is_first))
    def _():
        rim.wait_recv()

    gath = (gath_c, gath_s)

    def g_copy(part, r, kind, src, **dest):
        block = gath[part].at[pl.ds(r * G, G), lanes(src * C + c)]
        return pltpu.make_async_remote_copy(
            src_ref=block, dst_ref=block, send_sem=gs_sem.at[part, r, kind], recv_sem=gr_sem.at[part, r, kind],
            device_id=at(**dest), device_id_type=MESH,
        )

    def own(part, r, kind):
        return g_copy(part, r, kind, x, **({"x": right}, {"x": left}, {"core": other})[kind])

    def fwd(part, r, kind, odd):
        if kind == 5:
            return g_copy(part, r, 5, right, x=left) if odd else g_copy(part, r, 5, left, x=right)
        return g_copy(part, r, kind, {3: left, 4: right, 6: far}[kind], core=other)

    tap = taps[...].astype(f32)
    g_gain = group_gain[...]
    for k in range(NB):
        base = PAD + k * BIG
        total_c = (
            tap[0:1, :] * cin_v[pl.ds(base - 2, BIG), :]
            + tap[1:2, :] * cin_v[pl.ds(base - 1, BIG), :]
            + tap[2:3, :] * cin_v[pl.ds(base, BIG), :]
        )
        gated = pb_v[pl.ds(k * BIG, BIG), :] * total_c
        s = lax.rsqrt(jnp.mean(gated * gated, axis=-1, keepdims=True) + NORM_EPS)
        gath_c[pl.ds(k * BIG, BIG), lanes(me)] = (gated * s * g_gain).astype(bf16)
        for h in range(2):
            for kind in range(3):
                own(0, 2 * k + h, kind).start()

    for d in range(1, Z):
        @pl.when(z - d >= 0)
        def _():
            b_copy(d).wait_recv()

    def earlier(i, p):
        s, dec = piece(b_recv, i)
        return p * dec + s

    incoming = lax.fori_loop(0, z, earlier, jnp.zeros((Q, G), f32))
    for j in range(Y):
        c_src[j] = incoming.astype(bf16)
        if j < Y - 1:
            s, dec = piece(a_recv, j)
            incoming = incoming * dec + s
    mine = pl.ds(pl.multiple_of(y * Q, Q), Q)
    c_recv[mine, :] = c_src[y]

    def c_copy(d):
        t = lax.rem(y + d, Y)
        return pltpu.make_async_remote_copy(
            src_ref=c_src.at[t], dst_ref=c_recv.at[mine], send_sem=cs_sem.at[d], recv_sem=cr_sem.at[d],
            device_id=at(y=t), device_id_type=MESH,
        )

    for d in range(1, Y):
        c_copy(d).start()
    for d in range(1, Y):
        c_copy(d).wait_recv()

    s_gain = state_gain[...]
    before = c_recv[...].astype(f32)

    def cross(n, _):
        rows = pl.ds(pl.multiple_of(n * G, G), G)
        whole = prior_v[n] + before * offs_v[n, 0:1, :]
        read = oa_v[rows, :] + dot_nt(qin_v[rows, :], whole.astype(bf16))
        s = lax.rsqrt(jnp.mean(read * read, axis=-1, keepdims=True) + NORM_EPS)
        gath_s[rows, lanes(me)] = (read * s * s_gain * gate_v[rows, :]).astype(bf16)
        for kind in range(3):
            own(1, n, kind).start()
        return 0

    lax.fori_loop(0, N, cross, 0)

    def forward(part):
        def near(p, _):
            for e in range(2):
                r = 2 * p + e
                own(part, r, 0).wait_recv()
                if e == 0:
                    fwd(part, r, 5, e).start()
                fwd(part, r, 3, e).start()
                own(part, r, 1).wait_recv()
                if e == 1:
                    fwd(part, r, 5, e).start()
                fwd(part, r, 4, e).start()
            return 0

        lax.fori_loop(0, N // 2, near, 0)

    def distant(part, p):
        for e in range(2):
            fwd(part, 2 * p + e, 5, e).wait_recv()
            fwd(part, 2 * p + e, 6, e).start()

    def arrived(part, p):
        for e in range(2):
            r = 2 * p + e
            own(part, r, 2).wait_recv()
            for kind in (3, 4, 6):
                fwd(part, r, kind, e).wait_recv()

    for cp in own_in:
        cp.wait()
    forward(0)

    def far_c(p, _):
        distant(0, p)
        return 0

    lax.fori_loop(0, N // 2, far_c, 0)
    for d in range(1, TP):
        w_copy(1, d).wait_recv()
        w_copy(0, d).wait_recv()

    def conv_out(p, _):
        arrived(0, p)
        rows = pl.ds(pl.multiple_of(p * BIG, BIG), BIG)
        acc_v[rows, :] = dot(gath_c[rows, :], wcol_c[...])
        return 0

    lax.fori_loop(0, N // 2, conv_out, 0)
    forward(1)

    def far_s(p, _):
        distant(1, p)
        return 0

    lax.fori_loop(0, N // 2, far_s, 0)

    def result(p):
        rows = pl.ds(pl.multiple_of(p * BIG, BIG), BIG)
        return pltpu.make_async_copy(out_v.at[rows], out.at[rows], out_sem.at[p])

    def state_out(p, _):
        arrived(1, p)
        rows = pl.ds(pl.multiple_of(p * BIG, BIG), BIG)
        out_v[rows, :] = (acc_v[rows, :] + dot(gath_s[rows, :], wcol_s[...])).astype(bf16)
        result(p).start()
        return 0

    lax.fori_loop(0, N // 2, state_out, 0)

    def drain(p, _):
        for part in range(2):
            for e in range(2):
                r = 2 * p + e
                for kind in range(3):
                    own(part, r, kind).wait_send()
                for kind in range(3, 7):
                    fwd(part, r, kind, e).wait_send()
        result(p).wait()
        return 0

    lax.fori_loop(0, N // 2, drain, 0)
    for d in range(1, TP):
        w_copy(0, d).wait_send()
        w_copy(1, d).wait_send()
    for d in range(1, Y):
        a_copy(d).wait_send()
        c_copy(d).wait_send()
    for d in range(1, Z):
        @pl.when(z + d < Z)
        def _():
            b_copy(d).wait_send()

    @pl.when(jnp.logical_not(is_last))
    def _():
        rim.wait_send()


def solution(mesh):
    Y, X, C = 4, 4, 2
    Z = mesh.size // (Y * X * C)
    sizes = (Z, Y, X, C)
    split = Mesh(mesh.devices.reshape(sizes), ("z", "y", "x", "core"))
    SP, TPX = ("z", "y"), ("x", "core")

    def body(
        tokens, in_gain, w_query, w_forget, w_input, w_outgate, w_conv_h, w_conv_b, w_conv_c,
        forget_floor, forget_leak, state_gain, conv_taps, group_gain, out_state, out_conv,
    ):
        T, D = tokens.shape
        N, TP = T // G, X * C
        cols = out_state.shape[1] // TP
        Q = G // Y
        vmem, hbm = pl.BlockSpec(memory_space=pltpu.VMEM), pl.BlockSpec(memory_space=pl.ANY)
        dma = pltpu.SemaphoreType.DMA
        return pl.pallas_call(
            functools.partial(kernel, sizes),
            out_shape=jax.ShapeDtypeStruct((T, cols), bf16),
            in_specs=[hbm, vmem] + [hbm] * 7 + [vmem, hbm, vmem, vmem, vmem, hbm, hbm],
            out_specs=hbm,
            scratch_shapes=[
                pltpu.VMEM((T, D), bf16),
                pltpu.VMEM((D, 7 * G), bf16),
                pltpu.VMEM((T, G), f32),
                pltpu.VMEM((N, G, G), f32),
                pltpu.VMEM((N, 8, G), f32),
                pltpu.VMEM((T, G), bf16),
                pltpu.VMEM((T, G), f32),
                pltpu.VMEM((T, G), f32),
                pltpu.VMEM((T + PAD, G), f32),
                pltpu.VMEM((T, G), f32),
                pltpu.VMEM((T, TP * G), bf16),
                pltpu.VMEM((T, TP * G), bf16),
                pltpu.VMEM((TP * G, cols), bf16),
                pltpu.VMEM((TP * G, cols), bf16),
                pltpu.VMEM((T, cols), f32),
                pltpu.VMEM((T, cols), bf16),
                pltpu.VMEM((Y, Q + 16, G), bf16),
                pltpu.VMEM((Y, Q + 16, G), bf16),
                pltpu.VMEM((Q + 16, G), bf16),
                pltpu.VMEM((Z, Q + 16, G), bf16),
                pltpu.VMEM((Y, Q, G), bf16),
                pltpu.VMEM((G, G), bf16),
                dma((T // (2 * G),)), dma((7,)), dma, dma((2,)), dma((N // 2,)),
                dma((2, TP)), dma((2, TP)), dma((Y,)), dma((Y,)), dma((Z,)), dma((Z,)), dma((Y,)), dma((Y,)),
                dma((2,)), dma((2, N, 7)), dma((2, N, 7)),
            ],
            compiler_params=pltpu.CompilerParams(
                collective_id=0, has_side_effects=True, vmem_limit_bytes=60 * 1024 * 1024
            ),
            name="mixer_layer",
        )(
            tokens, in_gain.reshape(1, -1), w_query, w_forget, w_input, w_outgate, w_conv_h, w_conv_b, w_conv_c,
            forget_floor.reshape(1, -1), forget_leak, state_gain.reshape(1, -1), conv_taps,
            group_gain.reshape(1, -1), out_state, out_conv,
        )

    cut = P(None, TPX)
    placed = (
        P(SP, None), P(), cut, cut, cut, cut, cut, cut, cut, P(TPX), P(SP, TPX), P(), cut, P(),
        P(TPX, None), P(TPX, None),
    )
    return jax.shard_map(body, mesh=split, in_specs=placed, out_specs=P(SP, TPX), check_vma=False)
```

time: 187 us -> 58.6 us (0.31)
  blocking collectives: 66.6 us -> 0 us
  Pallas kernels: 0 us -> 56.5 us
  other arithmetic: 44.8 us -> 0 us
  matrix products: 38.1 us -> 0 us
  waiting for transfers between devices: 16.4 us -> 0 us
  between operations: 13.9 us -> 0.01 us
  starting transfers between devices: 4.02 us -> 0 us
    pallas_call x0 -> x1, Pallas kernels: none -> 56.5 us  [body(): pl.pallas_call(functools.partial(kernel, sizes), out_shape=jax.ShapeDtype...]
    dot_general x57 -> x0, matrix products: 38.1 us -> none  [the longest x7 14 us: project(): jnp.dot(normed, weight, preferred_element_type=jnp.float32)]
    all_to_all x1 -> x0, blocking collectives: 34.8 us -> none  [body(): lax.all_to_all(weight_rows, 'tp', split_axis=1, concat_axis=0, tiled=True)]
    all_gather x2 -> x0, blocking collectives: 31.9 us -> none  [collected_together(): both, at, found = (lax.all_gather(jnp.concatenate(lines), axis), 0, {})]
    dot_general x16 -> x0, other arithmetic: 27.3 us -> none  [state_block(): scores = jnp.einsum('hid,hjd,hijd->hij', query_blk, key_blk, decay_all)]
    all_gather x1 -> x0, waiting for transfers between devices: 16.3 us -> none  [body(): lax.all_gather(mixed_here, 'tp', axis=1, tiled=True)]
    exp x18 -> x0, other arithmetic: 9.81 us -> none  [the longest x16 9.79 us: state_block(): decay_all = jnp.exp(jnp.where(causal, diff_log, -jnp.inf))]
    ppermute x1 -> x0, starting transfers between devices: 4.02 us -> none  [from_behind(): return lax.ppermute(array, axis, pairs)]
  transfers between devices with their start and end apart: 2 -> 0, of which waited for: 1 -> 0; matrix products, arithmetic and copies ran while one was open for 38% -> 0% of each run, Pallas kernels for 0% -> 0%
where the time goes in v1:
time: 58.6 us; the launch traced here: 58.4 us
  Pallas kernels  56.5 us (96%)
  local copies, waits for them, and re-layouts  1.87 us (3%)
    pallas_call x1, Pallas kernels, body(): pl.pallas_call(functools.partial(kernel, sizes), out_shape=jax.ShapeDtype...  56.5 us
    unnamed x1, local copies, waits for them, and re-layouts  1.87 us

profile of v1, /device:TPU:1, one launch (start us, length us, event | category | flops | bytes accessed | tf_op | source)
XLA Modules:
  0.0 58.4 jit_solution(5828164685351111818)
XLA Ops:
  0.0 56.5 %mixer_layer.1 = bf16[1024,256]{1,0:T(8,128)(2,1)} custom-call(bf16[1024,2048]{1,0:T(8,128)(2,1)} %tokens.1, f32[1,2048]{1,0:T(1,128)} %bitcast.4, bf16[2048,128]{1,0:T(8,128)(2,1)} %w_query.1, bf16[2048,128]{1,0:T(8,128)(2,1)} %w_forget.1, bf16[2048,128]{1,0:T(8,128)(2,1)} %w_input.1, bf16[2048,128]{1,0:T(8,128)(2,1)} %w_outgate.1, ...), custom_call_target="tpu_custom_call" | custom-call | tf_op jit(solution)/shard_map/mixer_layer/pallas_call | solution.py:480
  56.5 1.9 %copy.18 = bf16[1024,256]{1,0:T(8,128)(2,1)} copy(bf16[1024,256]{1,0:T(8,128)(2,1)} %mixer_layer.1) | data formatting | bytes 1048576

commit v2 on v1

v2 whole, which is shorter than its diff:
```python
import functools

import jax
import jax.numpy as jnp
from jax import lax
from jax.experimental import pallas as pl
from jax.experimental.pallas import tpu as pltpu
from jax.sharding import Mesh
from jax.sharding import PartitionSpec as P

G = 128
PAD = 8
MEET = 3
NORM_EPS = 1e-06
MESH = pl.DeviceIdType.MESH
bf16, f32 = jnp.bfloat16, jnp.float32


def dot(a, b):
    return jnp.dot(a, b, preferred_element_type=f32)


def dot_nt(a, b):
    return lax.dot_general(a, b, (((1,), (1,)), ((), ())), preferred_element_type=f32)


def dot_tn(a, b):
    return lax.dot_general(a, b, (((0,), (0,)), ((), ())), preferred_element_type=f32)


def sigmoid(v):
    return 1.0 / (1.0 + jnp.exp(-v))


def rounded(v):
    return v.astype(bf16).astype(f32)


def split3(v):
    h1 = v.astype(bf16)
    r1 = v - h1.astype(f32)
    h2 = r1.astype(bf16)
    h3 = (r1 - h2.astype(f32)).astype(bf16)
    return h1, h2, h3


def kernel(
    sizes,
    tokens, gain_hbm, w_query, w_forget, w_input, w_outgate, w_conv_h, w_conv_b, w_conv_c,
    floor, leak, state_gain, taps, group_gain, out_state, out_conv,
    out,
    tok_v, norm_v, w_v, proj_v, cum_v, key_v, gain_v, scale_v, leak_v, prior_v, offs_v, qin_v, oa_v, gate_v, cin_v, pb_v,
    gath_c, gath_s, wcol_c, wcol_s, acc_v, out_v,
    a_src, a_recv, b_src, b_recv, c_src, c_recv,
    gain_sem, tok_sem, w_sem, leak_sem, own_sem, out_sem,
    ws_sem, wr_sem, ps_sem, pr_sem, as_sem, ar_sem, bs_sem, br_sem, cs_sem, cr_sem, rim_sem,
    gs_sem, gr_sem,
):
    Z, Y, X, C = sizes
    TP = X * C
    T = tok_v.shape[0]
    N = T // G
    BIG = 2 * G
    NB = T // BIG
    Q = G // Y
    COLS = out_v.shape[1]
    z, y, x, c = (lax.axis_index(n) for n in ("z", "y", "x", "core"))
    me = x * C + c
    other = 1 - c
    right, left = lax.rem(x + 1, X), lax.rem(x + X - 1, X)
    far = lax.rem(x + 2, X)

    def at(**kw):
        where = {"z": z, "y": y, "x": x, "core": c}
        where.update(kw)
        return (where["z"], where["y"], where["x"], where["core"])

    def side_by_side(ref, rows):
        return jnp.concatenate([ref[j, rows, :] for j in range(TP)], axis=1)

    tok_in = [
        pltpu.make_async_copy(tokens.at[pl.ds(k * BIG, BIG)], tok_v.at[pl.ds(k * BIG, BIG)], tok_sem.at[k])
        for k in range(NB)
    ]
    weights = (w_forget, w_input, w_query, w_outgate, w_conv_h, w_conv_c, w_conv_b)
    w_in = [
        pltpu.make_async_copy(w, w_v.at[:, pl.ds(k * G, G)], w_sem.at[k]) for k, w in enumerate(weights)
    ]
    leak_in = pltpu.make_async_copy(leak, leak_v, leak_sem)
    gain_in = pltpu.make_async_copy(gain_hbm, gain_v, gain_sem)
    gain_in.start()
    tok_in[0].start()
    for k in range(4):
        w_in[k].start()
    tok_in[1].start()
    leak_in.start()
    own_in = []
    for k, (src, dst) in enumerate(((out_state, wcol_s), (out_conv, wcol_c))):
        cp = pltpu.make_async_copy(
            src.at[:, pl.ds(pl.multiple_of(me * COLS, COLS), COLS)],
            dst.at[pl.ds(pl.multiple_of(me * G, G), G), :],
            own_sem.at[k],
        )
        cp.start()
        own_in.append(cp)

    barrier = pltpu.get_barrier_semaphore()
    for d in range(1, TP):
        t = lax.rem(me + d, TP)
        pl.semaphore_signal(barrier, inc=1, device_id=at(x=t // C, core=lax.rem(t, C)), device_id_type=MESH)
    for d in range(1, Y):
        pl.semaphore_signal(barrier, inc=1, device_id=at(y=lax.rem(y + d, Y)), device_id_type=MESH)
    for d in range(1, Z):
        pl.semaphore_signal(barrier, inc=1, device_id=at(z=lax.rem(z + d, Z)), device_id_type=MESH)
    last_y, first_y = y == Y - 1, y == 0

    @pl.when(last_y)
    def _():
        pl.semaphore_signal(barrier, inc=1, device_id=at(z=lax.rem(z + 1, Z), y=0), device_id_type=MESH)

    @pl.when(first_y)
    def _():
        pl.semaphore_signal(barrier, inc=1, device_id=at(z=lax.rem(z + Z - 1, Z), y=Y - 1), device_id_type=MESH)

    def norm_rows(k):
        for i in range(BIG // 64):
            rows = pl.ds(k * BIG + i * 64, 64)
            v = tok_v[rows, :].astype(f32)
            norm_v[rows, :] = (v * gain_v[...]).astype(bf16)
            s = lax.rsqrt(jnp.mean(v * v, axis=-1, keepdims=True) + NORM_EPS)
            scale_v[rows, :] = jnp.broadcast_to(s, (64, G))

    def project(k, lo, hi):
        big = pl.ds(k * BIG, BIG)
        acc = dot(norm_v[big, :], w_v[:, lo * G : hi * G])
        return [(acc[:, j * G : (j + 1) * G] * scale_v[big, :]).astype(bf16) for j in range(hi - lo)]

    gain_in.wait()
    tok_in[0].wait()
    for k in range(2, NB):
        tok_in[k].start()
    for k in range(4, 7):
        w_in[k].start()
    norm_rows(0)

    half = lax.rem(z, 2)
    HR = G // 2

    def w_copy(part, dx, core):
        src, dst = ((out_state, wcol_s), (out_conv, wcol_c))[part]
        to_x = lax.rem(x + dx, X)
        size = HR if dx else G
        skip = pl.multiple_of(half * HR, HR) if dx else 0
        return pltpu.make_async_remote_copy(
            src_ref=src.at[pl.ds(skip, size), pl.ds(pl.multiple_of((to_x * C + core) * COLS, COLS), COLS)],
            dst_ref=dst.at[pl.ds(pl.multiple_of(me * G + skip, HR), size), :],
            send_sem=ws_sem.at[part, dx * C + core],
            recv_sem=wr_sem.at[part, dx * C + c],
            device_id=at(x=to_x, core=core),
            device_id_type=MESH,
        )

    def w_wait(part, dx, core):
        dst = (wcol_s, wcol_c)[part]
        block = dst.at[pl.ds(0, HR if dx else G), :]
        pltpu.make_async_remote_copy(
            src_ref=block, dst_ref=block, send_sem=ws_sem.at[part, dx * C + core],
            recv_sem=wr_sem.at[part, dx * C + core], device_id=at(core=other), device_id_type=MESH,
        ).wait_recv()

    def w_pass(part, dx, core):
        dst = (wcol_s, wcol_c)[part]
        row = (lax.rem(x + X - dx, X) * C + core) * G
        block = dst.at[pl.ds(pl.multiple_of(row + half * HR, HR), HR), :]
        return pltpu.make_async_remote_copy(
            src_ref=block, dst_ref=block, send_sem=ps_sem.at[part, dx * C + core],
            recv_sem=pr_sem.at[part, dx * C + core], device_id=at(z=z + 1 - 2 * half), device_id_type=MESH,
        )

    fl = floor[...]
    row_i = lax.broadcasted_iota(jnp.int32, (G, G), 0)
    col_i = lax.broadcasted_iota(jnp.int32, (G, G), 1)
    lower = row_i >= col_i
    tri = jnp.where(lower, 1.0, 0.0).astype(bf16)

    def rec_proj(k):
        big = pl.ds(k * BIG, BIG)
        for j, p in enumerate(project(k, 0, 4)):
            proj_v[big, j * G : (j + 1) * G] = p

    state = jnp.zeros((G, G), f32)
    offset = jnp.zeros((1, G), f32)

    def gates(k, state, offset):
        for n in (2 * k, 2 * k + 1):
            rows = pl.ds(n * G, G)
            key = (1.0 - fl) * sigmoid(-proj_v[rows, 0:G].astype(f32))
            logf = jnp.log1p(-key) + leak_v[rows, :]
            h1, h2, h3 = split3(logf)
            cum3 = dot(tri, jnp.concatenate([h1, h2, h3], axis=1))
            cum = cum3[:, 0:G] + cum3[:, G : 2 * G] + cum3[:, 2 * G : 3 * G]
            last = cum[G - 1 : G, :]
            cum_v[rows, :] = cum
            key_v[rows, :] = key
            prior_v[n] = state
            offs_v[n] = jnp.broadcast_to(jnp.exp(offset), (8, G))
            k_last = (key * jnp.exp(last - cum)).astype(bf16)
            state = state * jnp.exp(last) + dot_tn(proj_v[rows, G : 2 * G], k_last)
            offset = offset + last
        return state, offset

    def inside(k):
        for n in (2 * k, 2 * k + 1):
            rows = pl.ds(n * G, G)
            cum = cum_v[rows, :]
            mid = cum[G // 2 - 1 : G // 2, :]
            pq = proj_v[rows, 2 * G : 3 * G].astype(f32)
            po = proj_v[rows, 3 * G : 4 * G].astype(f32)
            q_mid = pq * sigmoid(pq) * jnp.exp(cum - mid)
            k_mid = key_v[rows, :] * jnp.exp(mid - cum)
            scores = jnp.where(lower, dot_nt(q_mid.astype(bf16), k_mid.astype(bf16)), 0.0)
            oa_v[rows, :] = dot(scores.astype(bf16), proj_v[rows, G : 2 * G])
            qin_v[rows, :] = (q_mid * jnp.exp(mid)).astype(bf16)
            gate_v[rows, :] = po * sigmoid(po)

    def meet():
        count = TP - 1 + Y - 1 + Z - 1
        at_rim = jnp.logical_or(last_y, first_y)

        @pl.when(at_rim)
        def _():
            pl.semaphore_wait(barrier, count + 1)

        @pl.when(jnp.logical_not(at_rim))
        def _():
            pl.semaphore_wait(barrier, count)
        for part in (1, 0):
            for dx in range(1, X):
                for core in range(C):
                    w_copy(part, dx, core).start()
            w_copy(part, 0, other).start()

    for k in range(1, NB):
        tok_in[k].wait()
        if k == 1:
            for j in range(4):
                w_in[j].wait()
        if k == 2:
            leak_in.wait()
        norm_rows(k)
        rec_proj(k - 1)
        if k > 1:
            state, offset = gates(k - 2, state, offset)
        if k == MEET:
            meet()
    for j in range(4, 7):
        w_in[j].wait()
    rec_proj(NB - 1)
    state, offset = gates(NB - 2, state, offset)
    state, offset = gates(NB - 1, state, offset)
    if MEET == NB:
        meet()

    def decay_rows(decay):
        hi = decay.astype(bf16).astype(f32)
        r = lax.broadcasted_iota(jnp.int32, (16, G), 0)
        return jnp.where(r == 0, hi, jnp.where(r == 1, decay - hi, 0.0)).astype(bf16)

    def piece(ref, slot):
        block = ref[slot].astype(f32)
        return block[0:Q, :], block[Q : Q + 1, :] + block[Q + 1 : Q + 2, :]

    extra = decay_rows(jnp.exp(offset))
    for j in range(Y):
        a_src[j, 0:Q, :] = state[j * Q : (j + 1) * Q, :].astype(bf16)
        a_src[j, Q : Q + 16, :] = extra
    a_recv[y] = a_src[y]

    def a_copy(d):
        t = lax.rem(y + d, Y)
        return pltpu.make_async_remote_copy(
            src_ref=a_src.at[t], dst_ref=a_recv.at[y], send_sem=as_sem.at[d], recv_sem=ar_sem.at[d],
            device_id=at(y=t), device_id_type=MESH,
        )

    for d in range(1, Y):
        a_copy(d).start()

    gath = (gath_c, gath_s)

    def g_copy(part, r, kind, src, **dest):
        block = gath[part].at[src * C + c, pl.ds(r * G, G)]
        return pltpu.make_async_remote_copy(
            src_ref=block, dst_ref=block, send_sem=gs_sem.at[part, r, kind], recv_sem=gr_sem.at[part, r, kind],
            device_id=at(**dest), device_id_type=MESH,
        )

    def own(part, r, kind):
        return g_copy(part, r, kind, x, **({"x": right}, {"x": left}, {"core": other})[kind])

    def fwd(part, r, kind, odd):
        if kind == 5:
            return g_copy(part, r, 5, right, x=left) if odd else g_copy(part, r, 5, left, x=right)
        return g_copy(part, r, kind, {3: left, 4: right, 6: far}[kind], core=other)

    tap = taps[...].astype(f32)
    g_gain = group_gain[...]

    def conv_post(k):
        base = PAD + k * BIG
        total_c = (
            tap[0:1, :] * cin_v[pl.ds(base - 2, BIG), :]
            + tap[1:2, :] * cin_v[pl.ds(base - 1, BIG), :]
            + tap[2:3, :] * cin_v[pl.ds(base, BIG), :]
        )
        gated = pb_v[pl.ds(k * BIG, BIG), :] * total_c
        s = lax.rsqrt(jnp.mean(gated * gated, axis=-1, keepdims=True) + NORM_EPS)
        gath_c[me, pl.ds(k * BIG, BIG), :] = (gated * s * g_gain).astype(bf16)
        for h in range(2):
            for kind in range(3):
                own(0, 2 * k + h, kind).start()

    def conv_proj(k):
        big = pl.ds(k * BIG, BIG)
        ph, pc, pb = (p.astype(f32) for p in project(k, 4, 7))
        pb_v[big, :] = pb
        cin_v[pl.ds(PAD + k * BIG, BIG), :] = rounded(pc * ph)

    conv_proj(NB - 1)
    is_first = jnp.logical_and(z == 0, y == 0)
    is_last = jnp.logical_and(z == Z - 1, y == Y - 1)
    carry = lax.select(last_y, 1, 0)
    rim = pltpu.make_async_remote_copy(
        src_ref=cin_v.at[pl.ds(T, PAD)], dst_ref=cin_v.at[pl.ds(0, PAD)],
        send_sem=rim_sem.at[0], recv_sem=rim_sem.at[1],
        device_id=at(z=lax.rem(z + carry, Z), y=lax.rem(y + 1, Y)), device_id_type=MESH,
    )

    @pl.when(jnp.logical_not(is_last))
    def _():
        rim.start()

    @pl.when(is_first)
    def _():
        cin_v[0:PAD, :] = jnp.zeros((PAD, G), f32)

    conv_proj(0)
    conv_proj(1)
    conv_post(1)

    for d in range(1, Y):
        a_copy(d).wait_recv()
    total, total_d = piece(a_recv, 0)
    for j in range(1, Y):
        s, dec = piece(a_recv, j)
        total, total_d = total * dec + s, total_d * dec
    b_src[0:Q, :] = total.astype(bf16)
    b_src[Q : Q + 16, :] = decay_rows(total_d)

    def b_copy(d):
        return pltpu.make_async_remote_copy(
            src_ref=b_src, dst_ref=b_recv.at[z], send_sem=bs_sem.at[d], recv_sem=br_sem.at[d],
            device_id=at(z=lax.rem(z + d, Z)), device_id_type=MESH,
        )

    for d in range(1, Z):
        @pl.when(z + d < Z)
        def _():
            b_copy(d).start()

    for k in range(2, NB - 1):
        conv_proj(k)
        conv_post(k)
    conv_post(NB - 1)
    @pl.when(jnp.logical_not(is_first))
    def _():
        rim.wait_recv()

    conv_post(0)

    def in_turn(part, p):
        return p if part else lax.rem(p + 1, NB)

    def near(part, start, stop):
        def step(p, _):
            p = in_turn(part, p)
            for e in range(2):
                r = 2 * p + e
                own(part, r, 0).wait_recv()
                if e == 0:
                    fwd(part, r, 5, e).start()
                fwd(part, r, 3, e).start()
                own(part, r, 1).wait_recv()
                if e == 1:
                    fwd(part, r, 5, e).start()
                fwd(part, r, 4, e).start()
            return 0

        lax.fori_loop(start, stop, step, 0)

    def distant(part, p):
        for e in range(2):
            fwd(part, 2 * p + e, 5, e).wait_recv()
            fwd(part, 2 * p + e, 6, e).start()

    def arrived(part, p):
        for e in range(2):
            r = 2 * p + e
            own(part, r, 2).wait_recv()
            for kind in (3, 4, 6):
                fwd(part, r, kind, e).wait_recv()

    for k in range(NB):
        inside(k)

    for d in range(1, Z):
        @pl.when(z - d >= 0)
        def _():
            b_copy(d).wait_recv()

    def earlier(i, p):
        s, dec = piece(b_recv, i)
        return p * dec + s

    incoming = lax.fori_loop(0, z, earlier, jnp.zeros((Q, G), f32))
    for j in range(Y):
        c_src[j] = incoming.astype(bf16)
        if j < Y - 1:
            s, dec = piece(a_recv, j)
            incoming = incoming * dec + s
    mine = pl.ds(pl.multiple_of(y * Q, Q), Q)
    c_recv[mine, :] = c_src[y]

    def c_copy(d):
        t = lax.rem(y + d, Y)
        return pltpu.make_async_remote_copy(
            src_ref=c_src.at[t], dst_ref=c_recv.at[mine], send_sem=cs_sem.at[d], recv_sem=cr_sem.at[d],
            device_id=at(y=t), device_id_type=MESH,
        )

    for d in range(1, Y):
        c_copy(d).start()
    for part in (1, 0):
        for dx in range(1, X):
            for core in range(C):
                w_wait(part, dx, core)
                w_pass(part, dx, core).start()

    near(0, 0, NB // 2)
    for d in range(1, Y):
        c_copy(d).wait_recv()

    s_gain = state_gain[...]
    before = c_recv[...].astype(f32)

    for k in range(NB):
        for n in (2 * k, 2 * k + 1):
            rows = pl.ds(n * G, G)
            whole = prior_v[n] + before * offs_v[n, 0:1, :]
            read = oa_v[rows, :] + dot_nt(qin_v[rows, :], whole.astype(bf16))
            s = lax.rsqrt(jnp.mean(read * read, axis=-1, keepdims=True) + NORM_EPS)
            gath_s[me, rows, :] = (read * s * s_gain * gate_v[rows, :]).astype(bf16)
        for n in (2 * k, 2 * k + 1):
            for kind in range(3):
                own(1, n, kind).start()

    near(0, NB // 2, NB)
    near(1, 0, NB)

    def far_c(p, _):
        distant(0, in_turn(0, p))
        return 0

    lax.fori_loop(0, NB, far_c, 0)
    for cp in own_in:
        cp.wait()
    for part in range(2):
        w_wait(part, 0, other)
        for dx in range(1, X):
            for core in range(C):
                w_pass(part, dx, core).wait_recv()

    def conv_out(p, _):
        arrived(0, p)
        rows = pl.ds(pl.multiple_of(p * BIG, BIG), BIG)
        acc_v[rows, :] = dot(side_by_side(gath_c, rows), wcol_c[...])
        return 0

    lax.fori_loop(0, NB, conv_out, 0)

    def result(p):
        rows = pl.ds(pl.multiple_of(p * BIG, BIG), BIG)
        return pltpu.make_async_copy(out_v.at[rows], out.at[rows], out_sem.at[p])

    distant(1, 0)

    def state_out(p, _):
        @pl.when(p < NB - 1)
        def _():
            distant(1, p + 1)

        arrived(1, p)
        rows = pl.ds(pl.multiple_of(p * BIG, BIG), BIG)
        out_v[rows, :] = (acc_v[rows, :] + dot(side_by_side(gath_s, rows), wcol_s[...])).astype(bf16)
        result(p).start()
        return 0

    lax.fori_loop(0, NB, state_out, 0)

    def drain(p, _):
        for part in range(2):
            for e in range(2):
                r = 2 * p + e
                for kind in range(3):
                    own(part, r, kind).wait_send()
                for kind in range(3, 7):
                    fwd(part, r, kind, e).wait_send()
        result(p).wait()
        return 0

    lax.fori_loop(0, N // 2, drain, 0)
    for part in range(2):
        w_copy(part, 0, other).wait_send()
        for dx in range(1, X):
            for core in range(C):
                w_copy(part, dx, core).wait_send()
                w_pass(part, dx, core).wait_send()
    for d in range(1, Y):
        a_copy(d).wait_send()
        c_copy(d).wait_send()
    for d in range(1, Z):
        @pl.when(z + d < Z)
        def _():
            b_copy(d).wait_send()

    @pl.when(jnp.logical_not(is_last))
    def _():
        rim.wait_send()


def solution(mesh):
    Y, X, C = 4, 4, 2
    Z = mesh.size // (Y * X * C)
    sizes = (Z, Y, X, C)
    split = Mesh(mesh.devices.reshape(sizes), ("z", "y", "x", "core"))
    SP, TPX = ("z", "y"), ("x", "core")

    def body(
        tokens, in_gain, w_query, w_forget, w_input, w_outgate, w_conv_h, w_conv_b, w_conv_c,
        forget_floor, forget_leak, state_gain, conv_taps, group_gain, out_state, out_conv,
    ):
        T, D = tokens.shape
        N, TP = T // G, X * C
        cols = out_state.shape[1] // TP
        Q = G // Y
        vmem, hbm = pl.BlockSpec(memory_space=pltpu.VMEM), pl.BlockSpec(memory_space=pl.ANY)
        dma = pltpu.SemaphoreType.DMA
        return pl.pallas_call(
            functools.partial(kernel, sizes),
            out_shape=jax.ShapeDtypeStruct((T, cols), bf16),
            in_specs=[hbm, hbm] + [hbm] * 7 + [vmem, hbm, vmem, vmem, vmem, hbm, hbm],
            out_specs=hbm,
            scratch_shapes=[
                pltpu.VMEM((T, D), bf16),
                pltpu.VMEM((T, D), bf16),
                pltpu.VMEM((D, 7 * G), bf16),
                pltpu.VMEM((T, 4 * G), bf16),
                pltpu.VMEM((T, G), f32),
                pltpu.VMEM((T, G), f32),
                pltpu.VMEM((1, D), f32),
                pltpu.VMEM((T, G), f32),
                pltpu.VMEM((T, G), f32),
                pltpu.VMEM((N, G, G), f32),
                pltpu.VMEM((N, 8, G), f32),
                pltpu.VMEM((T, G), bf16),
                pltpu.VMEM((T, G), f32),
                pltpu.VMEM((T, G), f32),
                pltpu.VMEM((T + PAD, G), f32),
                pltpu.VMEM((T, G), f32),
                pltpu.VMEM((TP, T, G), bf16),
                pltpu.VMEM((TP, T, G), bf16),
                pltpu.VMEM((TP * G, cols), bf16),
                pltpu.VMEM((TP * G, cols), bf16),
                pltpu.VMEM((T, cols), f32),
                pltpu.VMEM((T, cols), bf16),
                pltpu.VMEM((Y, Q + 16, G), bf16),
                pltpu.VMEM((Y, Q + 16, G), bf16),
                pltpu.VMEM((Q + 16, G), bf16),
                pltpu.VMEM((Z, Q + 16, G), bf16),
                pltpu.VMEM((Y, Q, G), bf16),
                pltpu.VMEM((G, G), bf16),
                dma, dma((T // (2 * G),)), dma((7,)), dma, dma((2,)), dma((N // 2,)),
                dma((2, TP)), dma((2, TP)), dma((2, TP)), dma((2, TP)), dma((Y,)), dma((Y,)), dma((Z,)), dma((Z,)), dma((Y,)), dma((Y,)),
                dma((2,)), dma((2, N, 7)), dma((2, N, 7)),
            ],
            compiler_params=pltpu.CompilerParams(
                collective_id=0, has_side_effects=True, vmem_limit_bytes=60 * 1024 * 1024
            ),
            name="mixer_layer",
        )(
            tokens, in_gain.reshape(1, -1), w_query, w_forget, w_input, w_outgate, w_conv_h, w_conv_b, w_conv_c,
            forget_floor.reshape(1, -1), forget_leak, state_gain.reshape(1, -1), conv_taps,
            group_gain.reshape(1, -1), out_state, out_conv,
        )

    cut = P(None, TPX)
    placed = (
        P(SP, None), P(), cut, cut, cut, cut, cut, cut, cut, P(TPX), P(SP, TPX), P(), cut, P(),
        P(TPX, None), P(TPX, None),
    )
    return jax.shard_map(body, mesh=split, in_specs=placed, out_specs=P(SP, TPX), check_vma=False)
```

time: 58.6 us -> 44.8 us (0.76)
  Pallas kernels: 56.5 us -> 42.8 us
    pallas_call x1, Pallas kernels: 56.5 us -> 42.8 us  [body(): pl.pallas_call(functools.partial(kernel, sizes), out_shape=jax.ShapeDtype...]
where the time goes in v2:
time: 44.8 us; the launch traced here: 44.7 us
  Pallas kernels  42.8 us (96%)
  local copies, waits for them, and re-layouts  1.87 us (4%)
    pallas_call x1, Pallas kernels, body(): pl.pallas_call(functools.partial(kernel, sizes), out_shape=jax.ShapeDtype...  42.8 us
    unnamed x1, local copies, waits for them, and re-layouts  1.87 us

profile of v2, /device:TPU:1, one launch (start us, length us, event | category | flops | bytes accessed | tf_op | source)
XLA Modules:
  0.0 44.7 jit_solution(17723835753339114972)
XLA Ops:
  0.0 42.8 %mixer_layer.1 = bf16[1024,256]{1,0:T(8,128)(2,1)} custom-call(bf16[1024,2048]{1,0:T(8,128)(2,1)} %tokens.1, f32[1,2048]{1,0:T(1,128)} %bitcast.4, bf16[2048,128]{1,0:T(8,128)(2,1)} %w_query.1, bf16[2048,128]{1,0:T(8,128)(2,1)} %w_forget.1, bf16[2048,128]{1,0:T(8,128)(2,1)} %w_input.1, bf16[2048,128]{1,0:T(8,128)(2,1)} %w_outgate.1, ...), custom_call_target="tpu_custom_call" | custom-call | tf_op jit(solution)/shard_map/mixer_layer/pallas_call | solution.py:558
  42.8 1.9 %copy.18 = bf16[1024,256]{1,0:T(8,128)(2,1)} copy(bf16[1024,256]{1,0:T(8,128)(2,1)} %mixer_layer.1) | data formatting | bytes 1048576

commit v3 on v2

--- a/solution.py
+++ b/solution.py
@@ -46,13 +46,13 @@
 
 def kernel(
     sizes,
-    tokens, gain_hbm, w_query, w_forget, w_input, w_outgate, w_conv_h, w_conv_b, w_conv_c,
-    floor, leak, state_gain, taps, group_gain, out_state, out_conv,
-    out,
-    tok_v, norm_v, w_v, proj_v, cum_v, key_v, gain_v, scale_v, leak_v, prior_v, offs_v, qin_v, oa_v, gate_v, cin_v, pb_v,
-    gath_c, gath_s, wcol_c, wcol_s, acc_v, out_v,
+    tokens, w_query, w_forget, w_input, w_outgate, w_conv_h, w_conv_b, w_conv_c,
+    leak, small, out_state, out_conv,
+    out_v,
+    tok_v, norm_v, w_v, proj_v, cum_v, key_v, scale_v, leak_v, prior_v, offs_v, qin_v, oa_v, gate_v, cin_v, pb_v,
+    gath_c, gath_s, wcol_c, wcol_s, acc_v,
     a_src, a_recv, b_src, b_recv, c_src, c_recv,
-    gain_sem, tok_sem, w_sem, leak_sem, own_sem, out_sem,
+    tok_sem, w_sem, leak_sem, own_sem,
     ws_sem, wr_sem, ps_sem, pr_sem, as_sem, ar_sem, bs_sem, br_sem, cs_sem, cr_sem, rim_sem,
     gs_sem, gr_sem,
 ):
@@ -87,10 +87,8 @@
         pltpu.make_async_copy(w, w_v.at[:, pl.ds(k * G, G)], w_sem.at[k]) for k, w in enumerate(weights)
     ]
     leak_in = pltpu.make_async_copy(leak, leak_v, leak_sem)
-    gain_in = pltpu.make_async_copy(gain_hbm, gain_v, gain_sem)
-    gain_in.start()
     tok_in[0].start()
-    for k in range(4):
+    for k in range(2):
         w_in[k].start()
     tok_in[1].start()
     leak_in.start()
@@ -122,35 +120,35 @@
     def _():
         pl.semaphore_signal(barrier, inc=1, device_id=at(z=lax.rem(z + Z - 1, Z), y=Y - 1), device_id_type=MESH)
 
-    def norm_rows(k):
-        for i in range(BIG // 64):
-            rows = pl.ds(k * BIG + i * 64, 64)
+    def norm_rows(n):
+        for i in range(2):
+            rows = pl.ds(n * G + i * 64, 64)
             v = tok_v[rows, :].astype(f32)
-            norm_v[rows, :] = (v * gain_v[...]).astype(bf16)
+            norm_v[rows, :] = (v * gain_row).astype(bf16)
             s = lax.rsqrt(jnp.mean(v * v, axis=-1, keepdims=True) + NORM_EPS)
             scale_v[rows, :] = jnp.broadcast_to(s, (64, G))
 
-    def project(k, lo, hi):
-        big = pl.ds(k * BIG, BIG)
-        acc = dot(norm_v[big, :], w_v[:, lo * G : hi * G])
-        return [(acc[:, j * G : (j + 1) * G] * scale_v[big, :]).astype(bf16) for j in range(hi - lo)]
-
-    gain_in.wait()
+    def project(n, lo, hi):
+        rows = pl.ds(n * G, G)
+        acc = dot(norm_v[rows, :], w_v[:, lo * G : hi * G])
+        return [(acc[:, j * G : (j + 1) * G] * scale_v[rows, :]).astype(bf16) for j in range(hi - lo)]
+
+    gain_row = jnp.concatenate([small[6 + j : 7 + j, :] for j in range(tok_v.shape[1] // G)], axis=1)
     tok_in[0].wait()
     for k in range(2, NB):
         tok_in[k].start()
-    for k in range(4, 7):
+    for k in range(2, 7):
         w_in[k].start()
     norm_rows(0)
-
-    half = lax.rem(z, 2)
-    HR = G // 2
+    norm_rows(1)
+
+    HR = G // Y
 
     def w_copy(part, dx, core):
         src, dst = ((out_state, wcol_s), (out_conv, wcol_c))[part]
         to_x = lax.rem(x + dx, X)
         size = HR if dx else G
-        skip = pl.multiple_of(half * HR, HR) if dx else 0
+        skip = pl.multiple_of(y * HR, HR) if dx else 0
         return pltpu.make_async_remote_copy(
             src_ref=src.at[pl.ds(skip, size), pl.ds(pl.multiple_of((to_x * C + core) * COLS, COLS), COLS)],
             dst_ref=dst.at[pl.ds(pl.multiple_of(me * G + skip, HR), size), :],
@@ -168,60 +166,58 @@
             recv_sem=wr_sem.at[part, dx * C + core], device_id=at(core=other), device_id_type=MESH,
         ).wait_recv()
 
-    def w_pass(part, dx, core):
+    def w_pass(part, dx, core, dy):
         dst = (wcol_s, wcol_c)[part]
         row = (lax.rem(x + X - dx, X) * C + core) * G
-        block = dst.at[pl.ds(pl.multiple_of(row + half * HR, HR), HR), :]
+        block = dst.at[pl.ds(pl.multiple_of(row + y * HR, HR), HR), :]
+        k = (dy - 1) * TP + dx * C + core
         return pltpu.make_async_remote_copy(
-            src_ref=block, dst_ref=block, send_sem=ps_sem.at[part, dx * C + core],
-            recv_sem=pr_sem.at[part, dx * C + core], device_id=at(z=z + 1 - 2 * half), device_id_type=MESH,
-        )
-
-    fl = floor[...]
+            src_ref=block, dst_ref=block, send_sem=ps_sem.at[part, k], recv_sem=pr_sem.at[part, k],
+            device_id=at(y=lax.rem(y + dy, Y)), device_id_type=MESH,
+        )
+
+    fl = small[3:4, :]
     row_i = lax.broadcasted_iota(jnp.int32, (G, G), 0)
     col_i = lax.broadcasted_iota(jnp.int32, (G, G), 1)
     lower = row_i >= col_i
     tri = jnp.where(lower, 1.0, 0.0).astype(bf16)
 
-    def rec_proj(k):
-        big = pl.ds(k * BIG, BIG)
-        for j, p in enumerate(project(k, 0, 4)):
-            proj_v[big, j * G : (j + 1) * G] = p
+    def rec_proj(n, lo, hi):
+        for j, p in enumerate(project(n, lo, hi)):
+            proj_v[pl.ds(n * G, G), (lo + j) * G : (lo + j + 1) * G] = p
 
     state = jnp.zeros((G, G), f32)
     offset = jnp.zeros((1, G), f32)
 
-    def gates(k, state, offset):
-        for n in (2 * k, 2 * k + 1):
-            rows = pl.ds(n * G, G)
-            key = (1.0 - fl) * sigmoid(-proj_v[rows, 0:G].astype(f32))
-            logf = jnp.log1p(-key) + leak_v[rows, :]
-            h1, h2, h3 = split3(logf)
-            cum3 = dot(tri, jnp.concatenate([h1, h2, h3], axis=1))
-            cum = cum3[:, 0:G] + cum3[:, G : 2 * G] + cum3[:, 2 * G : 3 * G]
-            last = cum[G - 1 : G, :]
-            cum_v[rows, :] = cum
-            key_v[rows, :] = key
-            prior_v[n] = state
-            offs_v[n] = jnp.broadcast_to(jnp.exp(offset), (8, G))
-            k_last = (key * jnp.exp(last - cum)).astype(bf16)
-            state = state * jnp.exp(last) + dot_tn(proj_v[rows, G : 2 * G], k_last)
-            offset = offset + last
+    def gates(n, state, offset):
+        rows = pl.ds(n * G, G)
+        key = (1.0 - fl) * sigmoid(-proj_v[rows, 0:G].astype(f32))
+        logf = jnp.log1p(-key) + leak_v[rows, :]
+        h1, h2, h3 = split3(logf)
+        cum3 = dot(tri, jnp.concatenate([h1, h2, h3], axis=1))
+        cum = cum3[:, 0:G] + cum3[:, G : 2 * G] + cum3[:, 2 * G : 3 * G]
+        last = cum[G - 1 : G, :]
+        cum_v[rows, :] = cum
+        key_v[rows, :] = key
+        prior_v[n] = state
+        offs_v[n] = jnp.broadcast_to(jnp.exp(offset), (8, G))
+        k_last = (key * jnp.exp(last - cum)).astype(bf16)
+        state = state * jnp.exp(last) + dot_tn(proj_v[rows, G : 2 * G], k_last)
+        offset = offset + last
         return state, offset
 
-    def inside(k):
-        for n in (2 * k, 2 * k + 1):
-            rows = pl.ds(n * G, G)
-            cum = cum_v[rows, :]
-            mid = cum[G // 2 - 1 : G // 2, :]
-            pq = proj_v[rows, 2 * G : 3 * G].astype(f32)
-            po = proj_v[rows, 3 * G : 4 * G].astype(f32)
-            q_mid = pq * sigmoid(pq) * jnp.exp(cum - mid)
-            k_mid = key_v[rows, :] * jnp.exp(mid - cum)
-            scores = jnp.where(lower, dot_nt(q_mid.astype(bf16), k_mid.astype(bf16)), 0.0)
-            oa_v[rows, :] = dot(scores.astype(bf16), proj_v[rows, G : 2 * G])
-            qin_v[rows, :] = (q_mid * jnp.exp(mid)).astype(bf16)
-            gate_v[rows, :] = po * sigmoid(po)
+    def inside(n):
+        rows = pl.ds(n * G, G)
+        cum = cum_v[rows, :]
+        mid = cum[G // 2 - 1 : G // 2, :]
+        pq = proj_v[rows, 2 * G : 3 * G].astype(f32)
+        po = proj_v[rows, 3 * G : 4 * G].astype(f32)
+        q_mid = pq * sigmoid(pq) * jnp.exp(cum - mid)
+        k_mid = key_v[rows, :] * jnp.exp(mid - cum)
+        scores = jnp.where(lower, dot_nt(q_mid.astype(bf16), k_mid.astype(bf16)), 0.0)
+        oa_v[rows, :] = dot(scores.astype(bf16), proj_v[rows, G : 2 * G])
+        qin_v[rows, :] = (q_mid * jnp.exp(mid)).astype(bf16)
+        gate_v[rows, :] = po * sigmoid(po)
 
     def meet():
         count = TP - 1 + Y - 1 + Z - 1
@@ -243,21 +239,24 @@
     for k in range(1, NB):
         tok_in[k].wait()
         if k == 1:
-            for j in range(4):
+            for j in range(2):
                 w_in[j].wait()
         if k == 2:
             leak_in.wait()
-        norm_rows(k)
-        rec_proj(k - 1)
-        if k > 1:
-            state, offset = gates(k - 2, state, offset)
+        for h in range(2):
+            norm_rows(2 * k + h)
+            rec_proj(2 * (k - 1) + h, 0, 2)
+            if k > 1:
+                state, offset = gates(2 * (k - 2) + h, state, offset)
         if k == MEET:
             meet()
-    for j in range(4, 7):
+    for j in range(2, 7):
         w_in[j].wait()
-    rec_proj(NB - 1)
-    state, offset = gates(NB - 2, state, offset)
-    state, offset = gates(NB - 1, state, offset)
+    for h in range(2):
+        rec_proj(N - 2 + h, 0, 2)
+        state, offset = gates(N - 4 + h, state, offset)
+    for h in range(2):
+        state, offset = gates(N - 2 + h, state, offset)
     if MEET == NB:
         meet()
 
@@ -303,8 +302,8 @@
             return g_copy(part, r, 5, right, x=left) if odd else g_copy(part, r, 5, left, x=right)
         return g_copy(part, r, kind, {3: left, 4: right, 6: far}[kind], core=other)
 
-    tap = taps[...].astype(f32)
-    g_gain = group_gain[...]
+    tap = small[0:3, :]
+    g_gain = small[5:6, :]
 
     def conv_post(k):
         base = PAD + k * BIG
@@ -321,10 +320,10 @@
                 own(0, 2 * k + h, kind).start()
 
     def conv_proj(k):
-        big = pl.ds(k * BIG, BIG)
-        ph, pc, pb = (p.astype(f32) for p in project(k, 4, 7))
-        pb_v[big, :] = pb
-        cin_v[pl.ds(PAD + k * BIG, BIG), :] = rounded(pc * ph)
+        for n in (2 * k, 2 * k + 1):
+            ph, pc, pb = (p.astype(f32) for p in project(n, 4, 7))
+            pb_v[pl.ds(n * G, G), :] = pb
+            cin_v[pl.ds(PAD + n * G, G), :] = rounded(pc * ph)
 
     conv_proj(NB - 1)
     is_first = jnp.logical_and(z == 0, y == 0)
@@ -347,6 +346,10 @@
     conv_proj(0)
     conv_proj(1)
     conv_post(1)
+
+    for n in range(2):
+        rec_proj(n, 2, 4)
+        inside(n)
 
     for d in range(1, Y):
         a_copy(d).wait_recv()
@@ -410,9 +413,9 @@
             for kind in (3, 4, 6):
                 fwd(part, r, kind, e).wait_recv()
 
-    for k in range(NB):
-        inside(k)
-
+    for n in range(2, 6):
+        rec_proj(n, 2, 4)
+        inside(n)
     for d in range(1, Z):
         @pl.when(z - d >= 0)
         def _():
@@ -440,17 +443,20 @@
 
     for d in range(1, Y):
         c_copy(d).start()
+    for n in range(6, N):
+        rec_proj(n, 2, 4)
+        inside(n)
+    near(0, 0, NB)
+    for d in range(1, Y):
+        c_copy(d).wait_recv()
+
     for part in (1, 0):
         for dx in range(1, X):
             for core in range(C):
                 w_wait(part, dx, core)
-                w_pass(part, dx, core).start()
-
-    near(0, 0, NB // 2)
-    for d in range(1, Y):
-        c_copy(d).wait_recv()
-
-    s_gain = state_gain[...]
+                for dy in range(1, Y):
+                    w_pass(part, dx, core, dy).start()
+    s_gain = small[4:5, :]
     before = c_recv[...].astype(f32)
 
     for k in range(NB):
@@ -464,7 +470,6 @@
             for kind in range(3):
                 own(1, n, kind).start()
 
-    near(0, NB // 2, NB)
     near(1, 0, NB)
 
     def far_c(p, _):
@@ -478,31 +483,30 @@
         w_wait(part, 0, other)
         for dx in range(1, X):
             for core in range(C):
-                w_pass(part, dx, core).wait_recv()
+                for dy in range(1, Y):
+                    w_pass(part, dx, core, dy).wait_recv()
 
     def conv_out(p, _):
+        p = in_turn(0, p)
         arrived(0, p)
         rows = pl.ds(pl.multiple_of(p * BIG, BIG), BIG)
         acc_v[rows, :] = dot(side_by_side(gath_c, rows), wcol_c[...])
         return 0
 
-    lax.fori_loop(0, NB, conv_out, 0)
-
-    def result(p):
-        rows = pl.ds(pl.multiple_of(p * BIG, BIG), BIG)
-        return pltpu.make_async_copy(out_v.at[rows], out.at[rows], out_sem.at[p])
-
-    distant(1, 0)
+    def far_s(p, _):
+        distant(1, p)
+        return 0
+
+
+    lax.fori_loop(0, NB // 2, conv_out, 0)
+    lax.fori_loop(0, NB // 2, far_s, 0)
+    lax.fori_loop(NB // 2, NB, conv_out, 0)
+    lax.fori_loop(NB // 2, NB, far_s, 0)
 
     def state_out(p, _):
-        @pl.when(p < NB - 1)
-        def _():
-            distant(1, p + 1)
-
         arrived(1, p)
         rows = pl.ds(pl.multiple_of(p * BIG, BIG), BIG)
         out_v[rows, :] = (acc_v[rows, :] + dot(side_by_side(gath_s, rows), wcol_s[...])).astype(bf16)
-        result(p).start()
         return 0
 
     lax.fori_loop(0, NB, state_out, 0)
@@ -515,7 +519,6 @@
                     own(part, r, kind).wait_send()
                 for kind in range(3, 7):
                     fwd(part, r, kind, e).wait_send()
-        result(p).wait()
         return 0
 
     lax.fori_loop(0, N // 2, drain, 0)
@@ -524,7 +527,8 @@
         for dx in range(1, X):
             for core in range(C):
                 w_copy(part, dx, core).wait_send()
-                w_pass(part, dx, core).wait_send()
+                for dy in range(1, Y):
+                    w_pass(part, dx, core, dy).wait_send()
     for d in range(1, Y):
         a_copy(d).wait_send()
         c_copy(d).wait_send()
@@ -555,11 +559,13 @@
         Q = G // Y
         vmem, hbm = pl.BlockSpec(memory_space=pltpu.VMEM), pl.BlockSpec(memory_space=pl.ANY)
         dma = pltpu.SemaphoreType.DMA
+        rows = [a.astype(f32).reshape(-1, G) for a in (conv_taps, forget_floor, state_gain, group_gain, in_gain)]
+        small = jnp.concatenate(rows, axis=0)
         return pl.pallas_call(
             functools.partial(kernel, sizes),
             out_shape=jax.ShapeDtypeStruct((T, cols), bf16),
-            in_specs=[hbm, hbm] + [hbm] * 7 + [vmem, hbm, vmem, vmem, vmem, hbm, hbm],
-            out_specs=hbm,
+            in_specs=[hbm] * 9 + [vmem, hbm, hbm],
+            out_specs=vmem,
             scratch_shapes=[
                 pltpu.VMEM((T, D), bf16),
                 pltpu.VMEM((T, D), bf16),
@@ -567,7 +573,6 @@
                 pltpu.VMEM((T, 4 * G), bf16),
                 pltpu.VMEM((T, G), f32),
                 pltpu.VMEM((T, G), f32),
-                pltpu.VMEM((1, D), f32),
                 pltpu.VMEM((T, G), f32),
                 pltpu.VMEM((T, G), f32),
                 pltpu.VMEM((N, G, G), f32),
@@ -582,25 +587,23 @@
                 pltpu.VMEM((TP * G, cols), bf16),
                 pltpu.VMEM((TP * G, cols), bf16),
                 pltpu.VMEM((T, cols), f32),
-                pltpu.VMEM((T, cols), bf16),
                 pltpu.VMEM((Y, Q + 16, G), bf16),
                 pltpu.VMEM((Y, Q + 16, G), bf16),
                 pltpu.VMEM((Q + 16, G), bf16),
                 pltpu.VMEM((Z, Q + 16, G), bf16),
                 pltpu.VMEM((Y, Q, G), bf16),
                 pltpu.VMEM((G, G), bf16),
-                dma, dma((T // (2 * G),)), dma((7,)), dma, dma((2,)), dma((N // 2,)),
-                dma((2, TP)), dma((2, TP)), dma((2, TP)), dma((2, TP)), dma((Y,)), dma((Y,)), dma((Z,)), dma((Z,)), dma((Y,)), dma((Y,)),
+                dma((T // (2 * G),)), dma((7,)), dma, dma((2,)),
+                dma((2, TP)), dma((2, TP)), dma((2, (Y - 1) * TP)), dma((2, (Y - 1) * TP)), dma((Y,)), dma((Y,)), dma((Z,)), dma((Z,)), dma((Y,)), dma((Y,)),
                 dma((2,)), dma((2, N, 7)), dma((2, N, 7)),
             ],
             compiler_params=pltpu.CompilerParams(
-                collective_id=0, has_side_effects=True, vmem_limit_bytes=60 * 1024 * 1024
+                collective_id=0, has_side_effects=True, vmem_limit_bytes=56_000_000
             ),
             name="mixer_layer",
         )(
-            tokens, in_gain.reshape(1, -1), w_query, w_forget, w_input, w_outgate, w_conv_h, w_conv_b, w_conv_c,
-            forget_floor.reshape(1, -1), forget_leak, state_gain.reshape(1, -1), conv_taps,
-            group_gain.reshape(1, -1), out_state, out_conv,
+            tokens, w_query, w_forget, w_input, w_outgate, w_conv_h, w_conv_b, w_conv_c,
+            forget_leak, small, out_state, out_conv,
         )
 
     cut = P(None, TPX)

time: 44.8 us -> 42 us (0.938)
  Pallas kernels: 42.8 us -> 39.6 us
    pallas_call x1, Pallas kernels: 42.8 us -> 39.6 us  [body(): pl.pallas_call(functools.partial(kernel, sizes), out_shape=jax.ShapeDtype...]
    concatenate x0 -> x1, local copies, waits for them, and re-layouts: none -> 1.49 us  [body(): small = jnp.concatenate(rows, axis=0)]
    unnamed x1, local copies, waits for them, and re-layouts: 1.87 us -> 0.8 us
where the time goes in v3:
time: 42 us; the launch traced here: 41.9 us
  Pallas kernels  39.6 us (94%)
  local copies, waits for them, and re-layouts  2.29 us (5%)
    pallas_call x1, Pallas kernels, body(): pl.pallas_call(functools.partial(kernel, sizes), out_shape=jax.ShapeDtype...  39.6 us
    concatenate x1, local copies, waits for them, and re-layouts, body(): small = jnp.concatenate(rows, axis=0)  1.49 us

profile of v3, /device:TPU:1, one launch (start us, length us, event | category | flops | bytes accessed | tf_op | source)
XLA Modules:
  0.0 41.9 jit_solution(5455363601270671643)
XLA Ops:
  0.0 1.5 %concatenate.3.small = f32[22,128]{1,0:T(8,128)S(1)} concatenate(bf16[3,128]{1,0:T(4,128)(2,1)} %param.28, f32[1,128]{1,0:T(1,128)} %bitcast.5, f32[1,128]{1,0:T(1,128)} %bitcast.6, f32[1,128]{1,0:T(1,128)} %bitcast.7, f32[16,128]{1,0:T(8,128)} %bitcast.4), dimensions={0} | concatenate | bytes 21760 | tf_op jit(solution)/shard_map/concatenate | solution.py:563
  1.5 39.6 %mixer_layer.1 = bf16[1024,256]{1,0:T(8,128)(2,1)S(1)} custom-call(bf16[1024,2048]{1,0:T(8,128)(2,1)} %tokens.1, bf16[2048,128]{1,0:T(8,128)(2,1)} %w_query.1, bf16[2048,128]{1,0:T(8,128)(2,1)} %w_forget.1, bf16[2048,128]{1,0:T(8,128)(2,1)} %w_input.1, bf16[2048,128]{1,0:T(8,128)(2,1)} %w_outgate.1, bf16[2048,128]{1,0:T(8,128)(2,1)} %w_conv_h.1, ...), custom_call_target="tpu_custom_call" | custom-call | tf_op jit(solution)/shard_map/mixer_layer/pallas_call | solution.py:564
  41.1 0.8 %copy.18 = bf16[1024,256]{1,0:T(8,128)(2,1)} copy(bf16[1024,256]{1,0:T(8,128)(2,1)S(1)} %mixer_layer.1) | data formatting | bytes 1048576

commit v4 on v3

--- a/solution.py
+++ b/solution.py
@@ -10,7 +10,7 @@
 
 G = 128
 PAD = 8
-MEET = 3
+MEET = 4
 NORM_EPS = 1e-06
 MESH = pl.DeviceIdType.MESH
 bf16, f32 = jnp.bfloat16, jnp.float32
@@ -325,6 +325,9 @@
             pb_v[pl.ds(n * G, G), :] = pb
             cin_v[pl.ds(PAD + n * G, G), :] = rounded(pc * ph)
 
+    conv_proj(0)
+    conv_proj(1)
+    conv_post(1)
     conv_proj(NB - 1)
     is_first = jnp.logical_and(z == 0, y == 0)
     is_last = jnp.logical_and(z == Z - 1, y == Y - 1)
@@ -343,9 +346,10 @@
     def _():
         cin_v[0:PAD, :] = jnp.zeros((PAD, G), f32)
 
-    conv_proj(0)
-    conv_proj(1)
-    conv_post(1)
+    for k in range(2, NB - 1):
+        conv_proj(k)
+        conv_post(k)
+    conv_post(NB - 1)
 
     for n in range(2):
         rec_proj(n, 2, 4)
@@ -371,16 +375,9 @@
         def _():
             b_copy(d).start()
 
-    for k in range(2, NB - 1):
-        conv_proj(k)
-        conv_post(k)
-    conv_post(NB - 1)
-    @pl.when(jnp.logical_not(is_first))
-    def _():
-        rim.wait_recv()
-
-    conv_post(0)
-
+    for n in range(2, 4):
+        rec_proj(n, 2, 4)
+        inside(n)
     def in_turn(part, p):
         return p if part else lax.rem(p + 1, NB)
 
@@ -413,7 +410,7 @@
             for kind in (3, 4, 6):
                 fwd(part, r, kind, e).wait_recv()
 
-    for n in range(2, 6):
+    for n in range(4, 6):
         rec_proj(n, 2, 4)
         inside(n)
     for d in range(1, Z):
@@ -443,10 +440,16 @@
 
     for d in range(1, Y):
         c_copy(d).start()
+    @pl.when(jnp.logical_not(is_first))
+    def _():
+        rim.wait_recv()
+
+    conv_post(0)
+
     for n in range(6, N):
         rec_proj(n, 2, 4)
         inside(n)
-    near(0, 0, NB)
+    near(0, 0, NB - 1)
     for d in range(1, Y):
         c_copy(d).wait_recv()
 
@@ -470,6 +473,7 @@
             for kind in range(3):
                 own(1, n, kind).start()
 
+    near(0, NB - 1, NB)
     near(1, 0, NB)
 
     def far_c(p, _):

time: 42 us -> 40.8 us (0.971)
  Pallas kernels: 39.6 us -> 38.3 us
    pallas_call x1, Pallas kernels: 39.6 us -> 38.3 us  [body(): pl.pallas_call(functools.partial(kernel, sizes), out_shape=jax.ShapeDtype...]
where the time goes in v4:
time: 40.8 us; the launch traced here: 40.6 us
  Pallas kernels  38.3 us (94%)
  local copies, waits for them, and re-layouts  2.29 us (6%)
    pallas_call x1, Pallas kernels, body(): pl.pallas_call(functools.partial(kernel, sizes), out_shape=jax.ShapeDtype...  38.3 us
    concatenate x1, local copies, waits for them, and re-layouts, body(): small = jnp.concatenate(rows, axis=0)  1.49 us

profile of v4, /device:TPU:1, one launch (start us, length us, event | category | flops | bytes accessed | tf_op | source)
XLA Modules:
  0.0 40.6 jit_solution(15037886165557496642)
XLA Ops:
  0.0 1.5 %concatenate.3.small = f32[22,128]{1,0:T(8,128)S(1)} concatenate(bf16[3,128]{1,0:T(4,128)(2,1)} %param.28, f32[1,128]{1,0:T(1,128)} %bitcast.5, f32[1,128]{1,0:T(1,128)} %bitcast.6, f32[1,128]{1,0:T(1,128)} %bitcast.7, f32[16,128]{1,0:T(8,128)} %bitcast.4), dimensions={0} | concatenate | bytes 21760 | tf_op jit(solution)/shard_map/concatenate | solution.py:567
  1.5 38.3 %mixer_layer.1 = bf16[1024,256]{1,0:T(8,128)(2,1)S(1)} custom-call(bf16[1024,2048]{1,0:T(8,128)(2,1)} %tokens.1, bf16[2048,128]{1,0:T(8,128)(2,1)} %w_query.1, bf16[2048,128]{1,0:T(8,128)(2,1)} %w_forget.1, bf16[2048,128]{1,0:T(8,128)(2,1)} %w_input.1, bf16[2048,128]{1,0:T(8,128)(2,1)} %w_outgate.1, bf16[2048,128]{1,0:T(8,128)(2,1)} %w_conv_h.1, ...), custom_call_target="tpu_custom_call" | custom-call | tf_op jit(solution)/shard_map/mixer_layer/pallas_call | solution.py:568
  39.8 0.8 %copy.18 = bf16[1024,256]{1,0:T(8,128)(2,1)} copy(bf16[1024,256]{1,0:T(8,128)(2,1)S(1)} %mixer_layer.1) | data formatting | bytes 1048576

commit v5 on v4

--- a/solution.py
+++ b/solution.py
@@ -219,22 +219,24 @@
         qin_v[rows, :] = (q_mid * jnp.exp(mid)).astype(bf16)
         gate_v[rows, :] = po * sigmoid(po)
 
-    def meet():
-        count = TP - 1 + Y - 1 + Z - 1
-        at_rim = jnp.logical_or(last_y, first_y)
-
-        @pl.when(at_rim)
-        def _():
-            pl.semaphore_wait(barrier, count + 1)
-
-        @pl.when(jnp.logical_not(at_rim))
-        def _():
-            pl.semaphore_wait(barrier, count)
+    def send_weights():
         for part in (1, 0):
             for dx in range(1, X):
                 for core in range(C):
                     w_copy(part, dx, core).start()
             w_copy(part, 0, other).start()
+
+    def meet():
+        count = TP - 1 + Y - 1 + Z - 1
+        at_rim = jnp.logical_or(last_y, first_y)
+
+        @pl.when(at_rim)
+        def _():
+            pl.semaphore_wait(barrier, count + 1)
+
+        @pl.when(jnp.logical_not(at_rim))
+        def _():
+            pl.semaphore_wait(barrier, count)
 
     for k in range(1, NB):
         tok_in[k].wait()
@@ -284,6 +286,7 @@
 
     for d in range(1, Y):
         a_copy(d).start()
+    send_weights()
 
     gath = (gath_c, gath_s)
 
@@ -505,7 +508,6 @@
     lax.fori_loop(0, NB // 2, conv_out, 0)
     lax.fori_loop(0, NB // 2, far_s, 0)
     lax.fori_loop(NB // 2, NB, conv_out, 0)
-    lax.fori_loop(NB // 2, NB, far_s, 0)
 
     def state_out(p, _):
         arrived(1, p)
@@ -513,7 +515,12 @@
         out_v[rows, :] = (acc_v[rows, :] + dot(side_by_side(gath_s, rows), wcol_s[...])).astype(bf16)
         return 0
 
-    lax.fori_loop(0, NB, state_out, 0)
+    def far_then_out(p, _):
+        distant(1, p)
+        return state_out(p - NB // 2, 0)
+
+    lax.fori_loop(NB // 2, NB, far_then_out, 0)
+    lax.fori_loop(NB // 2, NB, state_out, 0)
 
     def drain(p, _):
         for part in range(2):

time: 40.8 us -> 41.1 us (level)
  no operation moved by 1% of the time
where the time goes in v5:
time: 41.1 us; the launch traced here: 40.9 us
  Pallas kernels  38.6 us (94%)
  local copies, waits for them, and re-layouts  2.29 us (6%)
    pallas_call x1, Pallas kernels, body(): pl.pallas_call(functools.partial(kernel, sizes), out_shape=jax.ShapeDtype...  38.6 us
    concatenate x1, local copies, waits for them, and re-layouts, body(): small = jnp.concatenate(rows, axis=0)  1.49 us

profile of v5, /device:TPU:1, one launch (start us, length us, event | category | flops | bytes accessed | tf_op | source)
XLA Modules:
  0.0 40.9 jit_solution(7653245249577491346)
XLA Ops:
  0.0 1.5 %concatenate.3.small = f32[22,128]{1,0:T(8,128)S(1)} concatenate(bf16[3,128]{1,0:T(4,128)(2,1)} %param.28, f32[1,128]{1,0:T(1,128)} %bitcast.5, f32[1,128]{1,0:T(1,128)} %bitcast.6, f32[1,128]{1,0:T(1,128)} %bitcast.7, f32[16,128]{1,0:T(8,128)} %bitcast.4), dimensions={0} | concatenate | bytes 21760 | tf_op jit(solution)/shard_map/concatenate | solution.py:574
  1.5 38.6 %mixer_layer.1 = bf16[1024,256]{1,0:T(8,128)(2,1)S(1)} custom-call(bf16[1024,2048]{1,0:T(8,128)(2,1)} %tokens.1, bf16[2048,128]{1,0:T(8,128)(2,1)} %w_query.1, bf16[2048,128]{1,0:T(8,128)(2,1)} %w_forget.1, bf16[2048,128]{1,0:T(8,128)(2,1)} %w_input.1, bf16[2048,128]{1,0:T(8,128)(2,1)} %w_outgate.1, bf16[2048,128]{1,0:T(8,128)(2,1)} %w_conv_h.1, ...), custom_call_target="tpu_custom_call" | custom-call | tf_op jit(solution)/shard_map/mixer_layer/pallas_call | solution.py:575
  40.1 0.8 %copy.18 = bf16[1024,256]{1,0:T(8,128)(2,1)} copy(bf16[1024,256]{1,0:T(8,128)(2,1)S(1)} %mixer_layer.1) | data formatting | bytes 1048576
